TPU v7x, 256 devices: a whole 4x4x8 slice. The times are simulated.
256 devices in a mesh: sp: 16 (over y, x), tp: 16 (over z, core).
Axes of the slice: x: 4, y: 4, z: 8, core: 2. Of those that a mesh axis runs over, the one named last changes fastest.
Arguments:
- saved_input: bfloat16 [4096, 2048], P('sp'), may hold values from -6 to 6
- cotangent: bfloat16 [4096, 2048], P('sp'), may hold values from -6 to 6
- expert_ids: int32 [4096, 2], P('sp'), may hold values from 0 to 15, all different within a row; in each aligned block of 256 rows (0 to 255, 256 to 511, ...) at most 64 rows name the same one
- route_weight: float32 [4096, 2], P('sp'), may hold values from 0.1 to 0.9
- w_gate: bfloat16 [16, 2048, 6144], P('sp', None, 'tp'), may hold values from -0.125 to 0.125
- w_up: bfloat16 [16, 2048, 6144], P('sp', None, 'tp'), may hold values from -0.125 to 0.125
- w_down: bfloat16 [16, 6144, 2048], P('sp', 'tp'), may hold values from -0.078125 to 0.078125
- w_out: bfloat16 [2048, 2048], P(None, 'tp'), may hold values from -0.125 to 0.125
- channel_gain: float32 [2048], P('tp'), may hold values from 0.1 to 1.9
- conv_taps: float32 [31, 2048], P(None, 'tp'), may hold values from -1 to 1
- glu_value: bfloat16 [2048, 4096], P('tp', 'sp'), may hold values from -6 to 6
- glu_gate: bfloat16 [2048, 4096], P('tp', 'sp'), may hold values from -8 to 8
- conv_out: bfloat16 [2048, 4096], P('tp', 'sp'), may hold values from -6 to 6
- norm_mean: float32 [4096], P('sp'), may hold values from -3 to 3
- norm_rstd: float32 [4096], P('sp'), may hold values from 0.5 to 2
Outputs:
- gate_grad: bfloat16 [16, 2048, 6144], P('sp', None, 'tp')
- up_grad: bfloat16 [16, 2048, 6144], P('sp', None, 'tp')
- down_grad: bfloat16 [16, 6144, 2048], P('sp', 'tp')
- proj_grad: float32 [2048, 2048], P('sp', 'tp')
- value_grad: bfloat16 [2048, 4096], P('tp', 'sp')
- gate_in_grad: bfloat16 [2048, 4096], P('tp', 'sp')
Inputs may be any that keep to these rules, and one draw needn't show every extreme that they name: `expert_ids`: the two experts of a position differ. In the positions of one block of 256, no expert is named more than 64 times, a bound that some block reaches.
All inputs are finite; a program needn't handle non-finite values.
Results may differ from a plain program's by a relative error of at most 0.018.
Values may be sent and summed in bfloat16 or wider, within the bound.
A program may use at most 128 MiB of HBM per device.

v0:
```python
import jax
import jax.numpy as jnp
from jax import lax
from jax.sharding import PartitionSpec as P

D = 2048
C = 2048


def in_one_piece(arrays, axis, split_dim, concat_dim, along):
    ends, at = ([], 0)
    for a in arrays[:-1]:
        at += a.shape[along]
        ends.append(at)
    both = jnp.concatenate(arrays, axis=along)
    return tuple(
        jnp.split(
            lax.all_to_all(both, axis, split_axis=split_dim, concat_axis=concat_dim, tiled=True),
            ends,
            axis=along,
        )
    )


def cut_along(value, dim, devices):
    before, after = (value.shape[:dim], value.shape[dim + 1 :])
    return jnp.moveaxis(value.reshape(*before, devices, -1, *after), dim, 0)


def sent_and_summed(value, axis, dim):
    devices = lax.axis_size(axis)
    tiles = lax.all_to_all(cut_along(value, dim, devices), axis, 0, 0, tiled=True)
    return jnp.sum(tiles.astype(jnp.float32), axis=0)


def copy_for_each(value, axis):
    copies = jnp.broadcast_to(value, (lax.axis_size(axis), *value.shape))
    return lax.all_to_all(copies, axis, split_axis=0, concat_axis=0, tiled=True)


def of_everyone(value, axis):
    everything = copy_for_each(value, axis)
    return jnp.sum(everything, axis=0)


def in_one(arrays, axis):
    ravelled, at, gathered = (jnp.concatenate([a.reshape(-1) for a in arrays]), 0, [])
    subtotal = of_everyone(ravelled, axis)
    for a in arrays:
        gathered.append(subtotal[at : at + a.size].reshape(a.shape))
        at += a.size
    return tuple(gathered)


def from_behind(value, axis, by):
    devices = lax.axis_size(axis)
    pairs = [(i, i + by) for i in range(devices) if 0 <= i + by < devices]
    return lax.ppermute(value, axis, pairs)


def contract(left, right, left_dim, right_dim):
    return lax.dot_general(
        left, right, (((left_dim,), (right_dim,)), ((), ())), preferred_element_type=jnp.float32
    )


def expert_grads(rows_in, rows_cot, gate_weight, up_weight, down_weight):
    gate_pre = jnp.dot(rows_in, gate_weight, preferred_element_type=jnp.float32)
    up_pre = jnp.dot(rows_in, up_weight, preferred_element_type=jnp.float32)
    sigma = jax.nn.sigmoid(gate_pre)
    hidden = (gate_pre * sigma * up_pre).astype(jnp.bfloat16)
    hidden_cot = contract(rows_cot, down_weight, 1, 1)
    down_part = contract(hidden, rows_cot, 0, 0).astype(jnp.bfloat16)
    gate_cot = (hidden_cot * up_pre * sigma * (1.0 + gate_pre * (1.0 - sigma))).astype(jnp.bfloat16)
    up_cot = (hidden_cot * gate_pre * sigma).astype(jnp.bfloat16)
    gate_part = contract(rows_in, gate_cot, 0, 0).astype(jnp.bfloat16)
    up_part = contract(rows_in, up_cot, 0, 0).astype(jnp.bfloat16)
    input_cot = contract(gate_cot, gate_weight, 1, 1) + contract(up_cot, up_weight, 1, 1)
    return (gate_part, up_part, down_part, input_cot)


def on_device(
    saved_input,
    cotangent,
    expert_ids,
    route_weight,
    w_gate,
    w_up,
    w_down,
    w_out,
    channel_gain,
    conv_taps,
    glu_value,
    glu_gate,
    conv_out,
    norm_mean,
    norm_rstd,
):
    tokens_here = cotangent.shape[0]
    sp_count = lax.axis_size("sp")
    local_experts = w_gate.shape[0]
    expert_count = local_experts * sp_count
    capacity = 4 * tokens_here // expert_count
    pairs = expert_ids.reshape(2 * tokens_here)
    onehot = (pairs[:, None] == jnp.arange(expert_count, dtype=jnp.int32)[None, :]).astype(
        jnp.int32
    )
    before = jnp.cumsum(onehot, axis=0) - onehot
    target = pairs * capacity + jnp.sum(before * onehot, axis=1)
    owner = (
        jnp.zeros((expert_count * capacity,), jnp.int32)
        .at[target]
        .set(jnp.arange(2 * tokens_here, dtype=jnp.int32) + 1)
    )
    filled = (owner > 0)[:, None]
    pair_index = jnp.maximum(owner - 1, 0)
    scaled = (route_weight[:, :, None] * cotangent.astype(jnp.float32)[:, None, :]).astype(
        jnp.bfloat16
    )
    scaled = scaled.reshape(2 * tokens_here, D)
    send_cot = jnp.where(filled, scaled[pair_index], jnp.zeros_like(scaled[:1])).reshape(
        expert_count, capacity, D
    )
    send_in = jnp.where(filled, saved_input[pair_index // 2], jnp.zeros_like(saved_input[:1]))
    send_in = send_in.reshape(expert_count, capacity, D)
    rows_cot, rows_in = in_one_piece((send_cot, send_in), "sp", 0, 1, 2)
    results = [expert_grads(rows_in[0], rows_cot[0], w_gate[0], w_up[0], w_down[0])]
    gate_grad = jnp.stack([result[0] for result in results])
    up_grad = jnp.stack([result[1] for result in results])
    down_grad = jnp.stack([result[2] for result in results])
    input_cot = jnp.stack([result[3] for result in results])
    blocks = input_cot.reshape(local_experts, sp_count, capacity, D)
    share = lax.psum_scatter(
        blocks.astype(jnp.bfloat16), "tp", scatter_dimension=2, tiled=True
    ).astype(jnp.float32)
    returned = lax.all_to_all(
        share.astype(jnp.bfloat16), "sp", split_axis=1, concat_axis=0, tiled=True
    ).astype(share.dtype)
    whole = lax.all_gather(returned.astype(jnp.bfloat16), "tp", axis=2, tiled=True).astype(
        returned.dtype
    )
    routed = whole.reshape(expert_count * capacity, D)[target].reshape(tokens_here, 2, D)
    summed = jnp.sum(routed, axis=1)
    mixed_cot = (cotangent.astype(jnp.float32) + summed).astype(jnp.bfloat16)
    centered = (conv_out.astype(jnp.float32) - norm_mean[None, :]) * norm_rstd[None, :]
    normed = centered * channel_gain[:, None]
    sigma = jax.nn.sigmoid(normed)
    output_act = (normed * sigma).astype(jnp.bfloat16)
    proj_grad = sent_and_summed(contract(mixed_cot, output_act, 0, 1).astype(jnp.bfloat16), "sp", 0)
    act_cot = contract(w_out, mixed_cot, 0, 1)
    norm_cot = act_cot * sigma * (1.0 + normed * (1.0 - sigma)) * channel_gain[:, None]
    first_sum, second_sum = in_one(
        (jnp.sum(norm_cot, axis=0), jnp.sum(norm_cot * centered, axis=0)), "tp"
    )
    conv_cot = norm_rstd[None, :] * (
        norm_cot - first_sum[None, :] / C - centered * second_sum[None, :] / C
    )
    reach = conv_taps.shape[0] - 1
    rim = from_behind(conv_cot[:, :reach], "sp", -1)
    padded = jnp.concatenate([conv_cot, rim], axis=1)
    glu_cot = conv_taps[0][:, None] * padded[:, :tokens_here]
    for lag in range(1, reach + 1):
        glu_cot = glu_cot + conv_taps[lag][:, None] * padded[:, lag : lag + tokens_here]
    gate_sigma = jax.nn.sigmoid(glu_gate.astype(jnp.float32))
    value_grad = (glu_cot * gate_sigma).astype(jnp.bfloat16)
    gate_in_grad = (
        glu_cot * glu_value.astype(jnp.float32) * gate_sigma * (1.0 - gate_sigma)
    ).astype(jnp.bfloat16)
    return (gate_grad, up_grad, down_grad, proj_grad, value_grad, gate_in_grad)


def solution(mesh):
    in_specs = (
        P("sp", None),
        P("sp", None),
        P("sp", None),
        P("sp", None),
        P("sp", None, "tp"),
        P("sp", None, "tp"),
        P("sp", "tp", None),
        P(None, "tp"),
        P("tp"),
        P(None, "tp"),
        P("tp", "sp"),
        P("tp", "sp"),
        P("tp", "sp"),
        P("sp"),
        P("sp"),
    )
    out_specs = (
        P("sp", None, "tp"),
        P("sp", None, "tp"),
        P("sp", "tp", None),
        P("sp", "tp"),
        P("tp", "sp"),
        P("tp", "sp"),
    )
    return jax.shard_map(
        on_device, mesh=mesh, in_specs=in_specs, out_specs=out_specs, check_vma=False
    )
```

profile of v0, /device:TPU:24, one launch (start us, length us, event | category | flops | bytes accessed | tf_op | source)
XLA Modules:
  0.0 370.5 jit_solution(13635867785435302561)
XLA Ops:
  7.2 0.0 copy-start
  7.2 0.0 reduce-scatter.2.cloned.1.call-start
  7.2 0.8 broadcast_multiply_fusion
  8.0 0.8 copy.65
  8.8 0.1 eq.25
  9.0 0.1 eq.29
  9.1 0.1 copy.64
  9.3 0.1 mul.436
  9.4 1.2 reduce-window.6
  10.6 0.2 slice_reduce_fusion
  10.9 0.1 fusion.114
  11.0 2.4 scatter_custom_fusion
  13.5 5.3 %mul.440 = f32[256,2,2048]{2,1,0:T(2,128)} broadcast(bf16[256,2048]{1,0:T(8,128)(2,1)} %param.16), dimensions={0,2} | broadcast | bytes 5242880 | tf_op jit(solution)/shard_map/mul | solution.py:117
  18.8 6.1 %mul.441 = f32[512,2048]{1,0:T(8,128)} reshape(f32[256,2,2048]{2,1,0:T(2,128)} %mul.440) | data formatting | bytes 8388608 | tf_op jit(solution)/shard_map/mul | solution.py:117
  24.9 0.1 copy.68
  25.0 0.1 mul.438
  25.2 0.1 broadcast_in_dim.46
  25.2 3.8 %multiply_convert_fusion = bf16[512,2048]{1,0:T(8,128)(2,1)} fusion(f32[512,2048]{1,0:T(8,128)} %mul.441, f32[512]{0:T(512)S(1)} %mul.438), kind=kLoop, calls=%fused_computation.8 | loop fusion | flops 2097152 | bytes 6293504 | tf_op jit(solution)/shard_map/convert_element_type | solution.py:117
  29.0 10.8 %gather_fusion = bf16[1024,2048]{1,0:T(8,128)(2,1)} fusion(bf16[512,2048]{1,0:T(8,128)(2,1)} %multiply_convert_fusion, s32[1024]{0:T(1024)S(1)} %get-tuple-element.73), kind=kCustom, calls=%fused_computation | custom fusion | bytes 8392704 | tf_op jit(solution)/shard_map/gather | solution.py:121
  39.8 6.0 %gather_fusion.1 = bf16[1024,2048]{1,0:T(8,128)(2,1)} fusion(bf16[256,2048]{1,0:T(8,128)(2,1)S(1)} %copy-done.2, s32[1024]{0:T(1024)S(1)} %get-tuple-element.74), kind=kCustom, calls=%fused_computation.1 | custom fusion | bytes 8392704 | tf_op jit(solution)/shard_map/gather | solution.py:124
  45.8 5.8 %broadcast_select_fusion.1 = (bf16[16,64,2048]{2,1,0:T(8,128)(2,1)}, bf16[16,64,2048]{2,1,0:T(8,128)(2,1)}) fusion(bf16[16,64,2048]{2,1,0:T(8,128)(2,1)} %bitcast.144, pred[16,64]{1,0:T(8,128)(4,1)S(1)} %broadcast_in_dim.46, bf16[16,64,2048]{2,1,0:T(8,128)(2,1)} %bitcast.145), kind=kLoop, calls=%fused_computation.10 | loop fusion | flops 4194304 | bytes 16778240 | tf_op jit(solution)/shard_map/jit(_where)/select_n | solution.py:121
  51.6 7.8 %pad_maximum_fusion = bf16[16,64,4096]{2,1,0:T(8,128)(2,1)} fusion(bf16[16,64,2048]{2,1,0:T(8,128)(2,1)} %get-tuple-element.78, bf16[16,64,2048]{2,1,0:T(8,128)(2,1)} %get-tuple-element.77), kind=kLoop, calls=%fused_computation.4 | loop fusion | flops 16777216 | bytes 16777216 | tf_op jit(solution)/shard_map/concatenate | solution.py:15
  59.4 100.8 %all_to_all.35 = bf16[16,64,4096]{2,1,0:T(8,128)(2,1)S(1)} all-to-all(bf16[16,64,4096]{2,1,0:T(8,128)(2,1)} %pad_maximum_fusion), channel_id=1, replica_groups=mesh['sp'=16,'tp'=16] {'sp'}, dimensions={0} | all-to-all | bytes 16777216 | tf_op jit(solution)/shard_map/all_to_all | solution.py:18
  160.3 2.3 fusion.3
  162.6 0.2 copy-done.5
  162.8 2.3 fusion.4
  165.2 0.2 copy-done.15
  165.4 2.8 multiply_convert_fusion.2
  168.2 2.4 fusion.8
  170.6 2.4 add_convert_fusion
  173.0 4.3 %copy.69 = bf16[1,16,64,2048]{3,1,0,2:T(8,128)(2,1)} copy(bf16[1,16,64,2048]{3,2,1,0:T(8,128)(2,1)S(1)} %bitcast.146) | data formatting | bytes 8388608 | tf_op jit(solution)/shard_map/convert_element_type | solution.py:134
  177.3 0.0 reduce-scatter.2.cloned.1.call-update
  177.3 0.0 all-gather.3.cloned.1.call-start
  177.3 64.5 %reduce-scatter.2.cloned.1.call-done = bf16[1,16,4,2048]{3,1,0,2:T(8,128)(2,1)} async-done(((bf16[1,16,64,2048]{3,1,0,2:T(8,128)(2,1)}), bf16[1,16,4,2048]{3,1,0,2:T(8,128)(2,1)}) %reduce-scatter.2.cloned.1.call-update) | async-done | bytes 262160 | tf_op jit(solution)/shard_map/reduce_scatter | solution.py:133
  241.9 1.2 copy.70
  243.0 13.6 %all_to_all.36 = bf16[1,16,4,2048]{3,2,0,1:T(4,128)(2,1)S(1)} all-to-all(bf16[1,16,4,2048]{3,2,0,1:T(4,128)(2,1)S(1)} %copy.70), channel_id=1, replica_groups=mesh['sp'=16,'tp'=16] {'sp'}, dimensions={1} | all-to-all | bytes 524288 | tf_op jit(solution)/shard_map/all_to_all | solution.py:136
  256.6 0.9 copy.71
  257.5 0.0 all-gather.3.cloned.1.call-update
  257.5 0.1 copy.73
  257.7 0.1 copy.76
  257.8 0.1 copy.75
  258.0 0.0 copy-start.19
  258.0 5.9 %fusion.5 = bf16[1,2048,384]{2,1,0:T(8,128)(2,1)} fusion(bf16[1024,384]{1,0:T(8,128)(2,1)S(1)} %get-tuple-element.41, bf16[1,1024,4096]{2,1,0:T(8,128)(2,1)} %bitcast.150), kind=kOutput, calls=%fused_computation.18 | convolution fusion | flops 1611399168 | bytes 6553600 | tf_op jit(solution)/shard_map/dot_general | solution.py:62
  263.9 5.4 %fusion.7 = bf16[1,384,2048]{2,1,0:T(8,128)(2,1)} fusion(bf16[1,1024,4096]{2,1,0:T(8,128)(2,1)} %bitcast.151, f32[1024,384]{1,0:T(8,128)S(1)} %copy-done.19, f32[1024,384]{1,0:T(8,128)S(1)} %copy-done.17), kind=kOutput, calls=%fused_computation.20 | convolution fusion | flops 1613758464 | bytes 8912896 | tf_op jit(solution)/shard_map/dot_general | solution.py:62
  269.3 26.8 %all-gather.3.cloned.1.call-done = bf16[1,16,64,2048]{3,1,0,2:T(8,128)(2,1)} async-done(((bf16[1,16,4,2048]{3,1,0,2:T(8,128)(2,1)}), bf16[1,16,64,2048]{3,1,0,2:T(8,128)(2,1)}) %all-gather.3.cloned.1.call-update) | async-done | bytes 4194320 | tf_op jit(solution)/shard_map/all_gather | solution.py:139
  296.1 7.8 %copy.72 = f32[1,16,64,2048]{3,2,1,0:T(8,128)} copy(bf16[1,16,64,2048]{3,1,0,2:T(8,128)(2,1)} %all-gather.3.cloned.1.call-done) | data formatting | bytes 12582912 | tf_op jit(solution)/shard_map/reshape | solution.py:142
  303.9 8.8 %gather_fusion.2 = f32[512,2048]{1,0:T(8,128)} fusion(f32[1024,2048]{1,0:T(8,128)} %bitcast.143, s32[1024]{0:T(1024)S(1)} %pad_clamp_fusion), kind=kCustom, calls=%fused_computation.2 | custom fusion | bytes 8390656 | tf_op jit(solution)/shard_map/gather | solution.py:142
  312.7 6.1 %reshape.159 = f32[256,2,2048]{2,1,0:T(2,128)} reshape(f32[512,2048]{1,0:T(8,128)} %gather_fusion.2) | data formatting | bytes 8388608 | tf_op jit(solution)/shard_map/reshape | solution.py:142
  318.7 0.0 copy-start.3
  318.8 0.0 copy-start.11
  318.8 8.6 %reduce_sum.58 = f32[256,2048]{1,0:T(8,128)} reduce(f32[256,2,2048]{2,1,0:T(2,128)} %reshape.159, f32[]{:T(128)} %constant.44.clone.1), dimensions={1}, to_apply=%region_5.6 | reduce | flops 524288 | bytes 6291460 | tf_op jit(solution)/shard_map/reduce_sum | solution.py:143
  327.5 2.1 fusion.123
  329.6 0.6 broadcast_in_dim.51
  330.3 4.4 %all-to-all-start.3 = ((f32[16,1,512]{2,1,0:T(1,128)}), f32[16,1,512]{2,1,0:T(1,128)S(1)}, u32[]{:S(2)}, u32[]{:S(2)}) async-start(f32[16,1,512]{2,1,0:T(1,128)} %broadcast_in_dim.51), calls=%async_computation.4 | async-start | bytes 65536 | tf_op jit(solution)/shard_map/all_to_all | solution.py:38
  334.6 3.1 convolution_convert_fusion.2
  337.7 4.6 %all-to-all-done.3 = f32[16,1,512]{2,1,0:T(1,128)S(1)} async-done(((f32[16,1,512]{2,1,0:T(1,128)}), f32[16,1,512]{2,1,0:T(1,128)S(1)}, u32[]{:S(2)}, u32[]{:S(2)}) %all-to-all-start.3) | async-done | bytes 32800 | tf_op jit(solution)/shard_map/all_to_all | solution.py:38
  342.3 7.2 %all-to-all-start.2 = ((bf16[16,128,128]{2,1,0:T(8,128)(2,1)}), bf16[16,128,128]{2,1,0:T(8,128)(2,1)S(1)}, u32[]{:S(2)}, u32[]{:S(2)}) async-start(bf16[16,128,128]{2,1,0:T(8,128)(2,1)} %bitcast.16), calls=%async_computation.3 | async-start | bytes 1048576 | tf_op jit(solution)/shard_map/all_to_all | solution.py:32
  349.6 0.2 subtract_multiply_fusion
  349.8 4.9 %collective-permute-start = (f32[128,30]{0,1:T(8,128)S(1)}, f32[128,30]{0,1:T(8,128)S(1)}, u32[]{:S(2)}, u32[]{:S(2)}) collective-permute-start(f32[128,30]{0,1:T(8,128)S(1)} %slice.271), channel_id=1, source_target_pairs={{16,0},{32,16},{48,32},{64,48},{80,64},{96,80},{112,96},{128,112},... | collective-permute-start | bytes 46088 | tf_op jit(solution)/shard_map/ppermute | solution.py:58
  354.7 5.8 %fusion.6 = bf16[1,2048,384]{2,1,0:T(8,128)(2,1)} fusion(bf16[1024,384]{1,0:T(8,128)(2,1)S(1)} %get-tuple-element.40, bf16[1,1024,4096]{2,1,0:T(8,128)(2,1)} %bitcast.152), kind=kOutput, calls=%fused_computation.19 | convolution fusion | flops 1611399168 | bytes 6553600 | tf_op jit(solution)/shard_map/dot_general | solution.py:62
  360.5 0.4 multiply_convert_fusion.5
  361.0 0.7 copy.77
  361.8 0.7 copy.78
  362.5 0.7 convert_reduce_fusion
  (51 shorter events, 0.3 us)
Async XLA Ops:
  7.2 153.1 %copy-start = (bf16[1,2048,384]{2,1,0:T(8,128)(2,1)S(1)}, bf16[1,2048,384]{2,1,0:T(8,128)(2,1)}, u32[]{:S(2)}) copy-start(bf16[1,2048,384]{2,1,0:T(8,128)(2,1)} %param.19) | copy-start | bytes 4718596
  7.2 234.7 %reduce-scatter.2.cloned.1.call-start = ((), (), s32[]{:S(2)}) async-start(), calls=%async_computation.5 | async-start | bytes 4456448 | tf_op jit(solution)/shard_map/reduce_scatter | solution.py:133
  18.8 6.1 %copy-start.13 = (f32[256,2]{0,1:T(2,128)S(1)}, f32[256,2]{0,1:T(2,128)}, u32[]{:S(2)}) copy-start(f32[256,2]{0,1:T(2,128)} %param.18) | copy-start | bytes 6148
  29.0 10.8 %copy-start.2 = (bf16[256,2048]{1,0:T(8,128)(2,1)S(1)}, bf16[256,2048]{1,0:T(8,128)(2,1)}, u32[]{:S(2)}) copy-start(bf16[256,2048]{1,0:T(8,128)(2,1)} %param.15) | copy-start | bytes 3145732
  160.3 4.9 %copy-start.4 = (bf16[16,64,4096]{2,1,0:T(8,128)(2,1)}, bf16[16,64,4096]{2,1,0:T(8,128)(2,1)S(1)}, u32[]{:S(2)}) copy-start(bf16[16,64,4096]{2,1,0:T(8,128)(2,1)S(1)} %all_to_all.35) | copy-start | bytes 25165828
  160.3 2.6 copy-start.5
  162.8 2.4 copy-start.16
  162.8 2.6 copy-start.15
  165.4 2.8 copy-start.18
  177.3 80.3 %copy-start.7 = (bf16[128,256]{1,0:T(8,128)(2,1)S(1)}, bf16[128,256]{1,0:T(8,128)(2,1)}, u32[]{:S(2)}) copy-start(bf16[128,256]{1,0:T(8,128)(2,1)} %param.27) | copy-start | bytes 196612
  177.3 80.4 %copy-start.8 = (bf16[128,256]{1,0:T(8,128)(2,1)S(1)}, bf16[128,256]{1,0:T(8,128)(2,1)}, u32[]{:S(2)}) copy-start(bf16[128,256]{1,0:T(8,128)(2,1)} %param.25) | copy-start | bytes 196612
  177.3 80.5 %copy-start.9 = (bf16[128,256]{1,0:T(8,128)(2,1)S(1)}, bf16[128,256]{1,0:T(8,128)(2,1)}, u32[]{:S(2)}) copy-start(bf16[128,256]{1,0:T(8,128)(2,1)} %param.26) | copy-start | bytes 196612
  177.3 80.7 %copy-start.10 = (f32[31,128]{1,0:T(8,128)S(1)}, f32[31,128]{1,0:T(8,128)}, u32[]{:S(2)}) copy-start(f32[31,128]{1,0:T(8,128)} %param.24) | copy-start | bytes 47620
  177.3 118.8 %all-gather.3.cloned.1.call-start = ((), (), s32[]{:S(2)}) async-start(), calls=%async_computation.6 | async-start | bytes 4456448 | tf_op jit(solution)/shard_map/all_gather | solution.py:139
  258.0 5.9 %copy-start.17 = (f32[1024,384]{1,0:T(8,128)S(1)}, f32[1024,384]{1,0:T(8,128)}, u32[]{:S(2)}) copy-start(f32[1024,384]{1,0:T(8,128)} %copy-done.16) | copy-start | bytes 4718596
  258.0 5.9 %copy-start.19 = (f32[1024,384]{1,0:T(8,128)S(1)}, f32[1024,384]{1,0:T(8,128)}, u32[]{:S(2)}) copy-start(f32[1024,384]{1,0:T(8,128)} %copy-done.18) | copy-start | bytes 4718596
  318.7 8.7 %copy-start.3 = (bf16[256,2048]{1,0:T(8,128)(2,1)S(1)}, bf16[256,2048]{1,0:T(8,128)(2,1)}, u32[]{:S(2)}) copy-start(bf16[256,2048]{1,0:T(8,128)(2,1)} %param.16) | copy-start | bytes 3145732
  318.8 8.7 %copy-start.6 = (bf16[2048,128]{1,0:T(8,128)(2,1)S(1)}, bf16[2048,128]{1,0:T(8,128)(2,1)}, u32[]{:S(2)}) copy-start(bf16[2048,128]{1,0:T(8,128)(2,1)} %param.22) | copy-start | bytes 1572868
  318.8 8.7 %copy-start.11 = (f32[256]{0:T(256)S(1)}, f32[256]{0:T(256)}, u32[]{:S(2)}) copy-start(f32[256]{0:T(256)} %param.29) | copy-start | bytes 3076
  318.8 8.7 %copy-start.12 = (f32[256]{0:T(256)S(1)}, f32[256]{0:T(256)}, u32[]{:S(2)}) copy-start(f32[256]{0:T(256)} %param.28) | copy-start | bytes 3076
  318.8 8.7 %copy-start.14 = (f32[128]{0:T(128)S(1)}, f32[128]{0:T(128)}, u32[]{:S(2)}) copy-start(f32[128]{0:T(128)} %param.23) | copy-start | bytes 1540
  330.3 12.1 %all-to-all-start.3 = ((f32[16,1,512]{2,1,0:T(1,128)}), f32[16,1,512]{2,1,0:T(1,128)S(1)}, u32[]{:S(2)}, u32[]{:S(2)}) async-start(f32[16,1,512]{2,1,0:T(1,128)} %broadcast_in_dim.51), calls=%async_computation.4 | async-start | bytes 65536 | tf_op jit(solution)/shard_map/all_to_all | solution.py:38
  342.3 20.2 %all-to-all-start.2 = ((bf16[16,128,128]{2,1,0:T(8,128)(2,1)}), bf16[16,128,128]{2,1,0:T(8,128)(2,1)S(1)}, u32[]{:S(2)}, u32[]{:S(2)}) async-start(bf16[16,128,128]{2,1,0:T(8,128)(2,1)} %bitcast.16), calls=%async_computation.3 | async-start | bytes 1048576 | tf_op jit(solution)/shard_map/all_to_all | solution.py:32
  349.8 10.7 %collective-permute-start = (f32[128,30]{0,1:T(8,128)S(1)}, f32[128,30]{0,1:T(8,128)S(1)}, u32[]{:S(2)}, u32[]{:S(2)}) collective-permute-start(f32[128,30]{0,1:T(8,128)S(1)} %slice.271), channel_id=1, source_target_pairs={{16,0},{32,16},{48,32},{64,48},{80,64},{96,80},{112,96},{128,112},... | collective-permute-start | bytes 46088 | tf_op jit(solution)/shard_map/ppermute | solution.py:58
  354.7 8.5 %copy-start.1 = (bf16[1,2048,384]{2,1,0:T(8,128)(2,1)S(1)}, bf16[1,2048,384]{2,1,0:T(8,128)(2,1)}, u32[]{:S(2)}) copy-start(bf16[1,2048,384]{2,1,0:T(8,128)(2,1)} %param.19) | copy-start | bytes 4718596
Sparse Core Ops, SparseCore 0:
  177.4 64.3 reduce-scatter.1
  257.6 38.3 all-gather.2
where the time goes:
time: 377 us; the launch traced here: 370 us
  blocking collectives  114 us (30%)
  waiting for transfers between devices  95.9 us (25%)
  local copies, waits for them, and re-layouts  64.6 us (17%)
  matrix products  34.5 us (9%)
  other arithmetic  29.5 us (8%)
  starting transfers between devices  16.5 us (4%)
  between operations  14.9 us (4%)
    all_to_all x1, blocking collectives, in_one_piece(): lax.all_to_all(both, axis, split_axis=split_dim, concat_axis=concat_dim,...  101 us
    reduce_scatter x1, waiting for transfers between devices, on_device(): lax.psum_scatter(blocks.astype(jnp.bfloat16), 'tp', scatter_dimension=2,...  64.5 us
    dot_general x8, matrix products, contract(): lax.dot_general(left, right, (((left_dim,), (right_dim,)), ((), ())), pre...  29.9 us
    all_gather x1, waiting for transfers between devices, on_device(): lax.all_gather(returned.astype(jnp.bfloat16), 'tp', axis=2, tiled=True)  26.8 us
    reshape x2, local copies, waits for them, and re-layouts, on_device(): whole.reshape(expert_count * capacity, D)[target].reshape(tokens_here, 2, D)  13.9 us
    all_to_all x1, blocking collectives, on_device(): lax.all_to_all(share.astype(jnp.bfloat16), 'sp', split_axis=1, concat_axi...  13.6 us
    mul x3, local copies, waits for them, and re-layouts, on_device(): route_weight[:, :, None] * cotangent.astype(jnp.float32)[:, None, :]  11.6 us
    gather x1, local copies, waits for them, and re-layouts, on_device(): scaled[pair_index]  10.8 us
  transfers between devices with their start and end apart: 5, of which 3 were waited for; matrix products, arithmetic and copies ran while one was open for 6% of the time, Pallas kernels for 0%

commit v1 on v0

v1 whole, which is shorter than its diff:
```python
import functools

import jax
import jax.numpy as jnp
from jax import lax
from jax.experimental import pallas as pl
from jax.experimental.pallas import tpu as pltpu
from jax.sharding import PartitionSpec as P

D = 2048
C = 2048
SIDE = 4
RING = 8
CAP = 64
BF16 = jnp.bfloat16
F32 = jnp.float32
MESH = pl.DeviceIdType.MESH

FAR = ((0, 2), (2, 0), (1, 2), (3, 2), (2, 1), (2, 3), (2, 2))
NEAR = ((0, 1), (0, 3), (1, 0), (3, 0), (1, 1), (1, 3), (3, 1), (3, 3))
OFFSETS = FAR + NEAR + ((0, 0),)
HALVES = ((0, 4), (4, 3))


def sp_at(dy, dx):
    sp = lax.axis_index("sp")
    y, x = sp // SIDE, sp % SIDE
    return ((y + dy) % SIDE) * SIDE + (x + dx) % SIDE


def contract(left, right, left_dim, right_dim):
    return lax.dot_general(
        left, right, (((left_dim,), (right_dim,)), ((), ())), preferred_element_type=F32
    )


def greet(others):
    barrier = pltpu.get_barrier_semaphore()
    for device in others:
        pl.semaphore_signal(barrier, inc=1, device_id=device, device_id_type=MESH)
    pl.semaphore_wait(barrier, len(others))


def group(with_sp):
    sp, tp = lax.axis_index("sp"), lax.axis_index("tp")
    z, core = tp // 2, tp % 2
    partner = (sp, z * 2 + 1 - core)
    up = (sp, ((z + 1) % RING) * 2 + core)
    down = (sp, ((z + RING - 1) % RING) * 2 + core)
    others = [partner, up, down]
    if with_sp:
        others += [(sp_at(dy, dx), tp) for dy, dx in OFFSETS[:-1]]
    return sp, tp, z, core, partner, up, down, others


class Copies:
    def __init__(self):
        self.started = []

    def send(self, src, dst, send_sem, recv_sem, device):
        copy = pltpu.make_async_remote_copy(
            src_ref=src,
            dst_ref=dst,
            send_sem=send_sem,
            recv_sem=recv_sem,
            device_id=device,
            device_id_type=MESH,
        )
        copy.start()
        self.started.append(copy)

    def arrived(self, dst, send_sem, recv_sem, device):
        pltpu.make_async_remote_copy(
            src_ref=dst,
            dst_ref=dst,
            send_sem=send_sem,
            recv_sem=recv_sem,
            device_id=device,
            device_id_type=MESH,
        ).wait_recv()

    def finish(self):
        for copy in self.started:
            copy.wait_send()


def select_kernel(ids_ref, weight_ref, in_ref, cot_ref, x_ref, row_ref, src0, src1):
    core = lax.axis_index("tp") % 2
    sp = lax.axis_index("sp")
    y, x = sp // SIDE, sp % SIDE
    tokens = in_ref.shape[0]
    lanes = lax.broadcasted_iota(jnp.int32, (tokens, 128), 1)
    one = [(ids_ref[:, k : k + 1] == lanes).astype(F32) for k in range(2)]
    count = (one[0] + one[1]).astype(BF16)
    earlier = (
        lax.broadcasted_iota(jnp.int32, (tokens, tokens), 0)
        > lax.broadcasted_iota(jnp.int32, (tokens, tokens), 1)
    ).astype(BF16)
    before = jnp.dot(earlier, count, preferred_element_type=F32)
    place = jnp.zeros((1, 128), jnp.int32)
    lane = lax.broadcasted_iota(jnp.int32, (1, 128), 1)
    for o, (dy, dx) in enumerate(OFFSETS):
        expert = ((y + dy) % SIDE) * SIDE + (x + dx) % SIDE
        place = jnp.where(lane == expert, o * CAP, place)
    row_of = before + place.astype(F32)
    rows = [
        jnp.sum(one[k] * row_of, axis=1, keepdims=True).astype(jnp.int32) for k in range(2)
    ]
    for k in range(2):
        row_ref[:, k : k + 1] = rows[k]
    cot = cot_ref[...].astype(F32)
    for k, src in enumerate((src0, src1)):
        scaled = (weight_ref[:, k : k + 1] * cot).astype(BF16)
        src[...] = jnp.where(core == 0, in_ref[...], scaled)

    def step(o, carry):
        at = lax.broadcasted_iota(jnp.int32, (tokens, 2 * CAP), 1) + o * (2 * CAP)
        total = contract((rows[0] == at).astype(BF16), src0[...], 0, 0) + contract(
            (rows[1] == at).astype(BF16), src1[...], 0, 0
        )
        x_ref[pl.ds(2 * o, 2)] = total.astype(BF16).reshape(2, RING, 8, D)
        return carry

    lax.fori_loop(0, len(OFFSETS) // 2, step, 0)


def select(ids, weight, rows_in, rows_cot):
    tokens = rows_in.shape[0]
    vmem = pl.BlockSpec(memory_space=pltpu.VMEM)
    return pl.pallas_call(
        select_kernel,
        out_shape=(
            jax.ShapeDtypeStruct((len(OFFSETS), RING, 8, D), BF16),
            jax.ShapeDtypeStruct((tokens, 2), jnp.int32),
        ),
        in_specs=[vmem] * 4,
        out_specs=(vmem, vmem),
        scratch_shapes=[pltpu.VMEM((tokens, D), BF16)] * 2,
        compiler_params=pltpu.CompilerParams(vmem_limit_bytes=24 << 20),
        name="select",
    )(ids, weight, rows_in, rows_cot)


def dispatch_kernel(
    x_ref,
    r_ref,
    far_send,
    far_recv,
    near_send,
    near_recv,
    up_send,
    up_recv,
    down_send,
    down_recv,
    share_send,
    share_recv,
    near_share_send,
    near_share_recv,
    local_sem,
):
    sp, tp, z, core, partner, up, down, others = group(True)
    copies = Copies()
    near_at = len(FAR)
    local_at = len(OFFSETS) - 1
    greet(others)

    def far(c, g, half):
        start, size = HALVES[half]
        return r_ref.at[c, pl.ds(start, size), g]

    for half, (start, size) in enumerate(HALVES):
        for o in range(start, start + size):
            copies.send(
                x_ref.at[o, z],
                r_ref.at[core, o, z],
                far_send.at[o],
                far_recv.at[o],
                (sp_at(*FAR[o]), tp),
            )
    for i, offset in enumerate(NEAR):
        copies.send(
            x_ref.at[near_at + i],
            r_ref.at[core, near_at + i],
            near_send.at[i],
            near_recv.at[i],
            (sp_at(*offset), tp),
        )
    n_near = len(NEAR)
    copies.send(
        x_ref.at[local_at],
        r_ref.at[core, local_at],
        near_share_send.at[n_near],
        near_share_recv.at[n_near],
        partner,
    )
    local = pltpu.make_async_copy(x_ref.at[local_at], r_ref.at[core, local_at], local_sem)
    local.start()

    def spread(g, k, half, going_up, going_down, slot):
        block = far(core, g, half)
        if going_up:
            copies.send(block, block, up_send.at[k, half], up_recv.at[k, half], up)
        if going_down:
            copies.send(block, block, down_send.at[k, half], down_recv.at[k, half], down)
        copies.send(block, block, share_send.at[slot, half], share_recv.at[slot, half], partner)

    for half, (start, size) in enumerate(HALVES):
        for o in range(start, start + size):
            copies.arrived(r_ref.at[core, o, z], far_send.at[o], far_recv.at[o], partner)
        spread(z, 0, half, True, True, 0)

    for k in range(1, 5):
        above, below = (z + RING - k) % RING, (z + k) % RING
        for half in range(2):
            if k < 4 or half == 0:
                copies.arrived(
                    far(core, above, half), up_send.at[k - 1, half], up_recv.at[k - 1, half], up
                )
                spread(above, k, half, k < 3 or (k == 3 and half == 0), False, k)
            if k < 4 or half == 1:
                copies.arrived(
                    far(core, below, half),
                    down_send.at[k - 1, half],
                    down_recv.at[k - 1, half],
                    down,
                )
                spread(below, k, half, False, k < 3 or (k == 3 and half == 1), 4 if k == 4 else 4 + k)
        for i in (2 * k - 2, 2 * k - 1):
            block = r_ref.at[core, near_at + i]
            copies.arrived(block, near_send.at[i], near_recv.at[i], partner)
            copies.send(block, block, near_share_send.at[i], near_share_recv.at[i], partner)

    for slot in range(RING):
        g = (z + RING - slot) % RING if slot <= 4 else (z + slot - 4) % RING
        for half in range(2):
            copies.arrived(
                far(1 - core, g, half),
                share_send.at[slot, half],
                share_recv.at[slot, half],
                partner,
            )
    for i in range(n_near + 1):
        copies.arrived(
            r_ref.at[1 - core, near_at + i], near_share_send.at[i], near_share_recv.at[i], partner
        )
    local.wait()
    copies.finish()


def dispatch(x):
    dma = pltpu.SemaphoreType.DMA
    n_near = len(NEAR)
    return pl.pallas_call(
        dispatch_kernel,
        out_shape=jax.ShapeDtypeStruct((2, *x.shape), BF16),
        in_specs=[pl.BlockSpec(memory_space=pltpu.VMEM)],
        out_specs=pl.BlockSpec(memory_space=pl.ANY),
        scratch_shapes=[
            dma((len(FAR),)),
            dma((len(FAR),)),
            dma((n_near,)),
            dma((n_near,)),
            dma((4, 2)),
            dma((4, 2)),
            dma((4, 2)),
            dma((4, 2)),
            dma((RING, 2)),
            dma((RING, 2)),
            dma((n_near + 1,)),
            dma((n_near + 1,)),
            dma,
        ],
        compiler_params=pltpu.CompilerParams(
            collective_id=0, has_side_effects=True, vmem_limit_bytes=24 << 20
        ),
        name="dispatch",
    )(x)


def input_kernel(gate_ref, up_ref, wg_ref, wu_ref, out_ref):
    total = contract(gate_ref[...], wg_ref[...], 1, 1) + contract(up_ref[...], wu_ref[...], 1, 1)
    total = total.astype(BF16)
    out_ref[0, 0] = total[:, :128]
    out_ref[1, 0] = total[:, 128:]


def input_shares(gate_cot, up_cot, w_gate, w_up):
    rows, hidden = gate_cot.shape
    whole = pl.BlockSpec((rows, hidden), lambda i: (0, 0))
    part = pl.BlockSpec((256, hidden), lambda i: (i, 0))
    return pl.pallas_call(
        input_kernel,
        grid=(RING,),
        out_shape=jax.ShapeDtypeStruct((2, RING, rows, 128), BF16),
        in_specs=[whole, whole, part, part],
        out_specs=pl.BlockSpec((2, 1, rows, 128), lambda i: (0, i, 0, 0)),
        compiler_params=pltpu.CompilerParams(vmem_limit_bytes=24 << 20),
        name="input_shares",
    )(gate_cot, up_cot, w_gate, w_up)


def collect_kernel(
    p_ref,
    row_ref,
    cot_ref,
    m_ref,
    pair_buf,
    out_up,
    in_up,
    out_down,
    in_down,
    sums,
    slots,
    cot_buf,
    mixed,
    pair_send,
    pair_recv,
    up_send,
    up_recv,
    down_send,
    down_recv,
    back_send,
    back_recv,
    gup_send,
    gup_recv,
    gdown_send,
    gdown_recv,
    share_send,
    share_recv,
    local_sem,
):
    sp, tp, z, core, partner, up, down, others = group(True)
    rows = p_ref.shape[2]
    tokens = m_ref.shape[0]
    half_rows = rows // 2
    half_tokens = tokens // 2
    copies = Copies()
    greet(others)
    order = (4, 3, -3, 2, -2, 1, -1, 0)
    for i, d in enumerate(order):
        g = (z + RING + d) % RING
        copies.send(
            p_ref.at[1 - core, g], pair_buf.at[g], pair_send.at[i], pair_recv.at[i], partner
        )
    fetch = pltpu.make_async_copy(
        cot_ref.at[:, pl.ds(pl.multiple_of(tp * 128, 128), 128)], cot_buf, local_sem.at[0]
    )
    fetch.start()

    def paired(d):
        i = order.index(d)
        g = (z + RING + d) % RING
        copies.arrived(pair_buf.at[g], pair_send.at[i], pair_recv.at[i], partner)

    def span(half):
        return pl.ds(half * half_rows, half_rows)

    def own(d, half):
        g = (z + RING + d) % RING
        return p_ref[core, g, span(half), :].astype(F32) + pair_buf[g, span(half), :].astype(F32)

    def go_up(hop, half):
        copies.send(
            out_up.at[hop, span(half)],
            in_up.at[hop, span(half)],
            up_send.at[hop, half],
            up_recv.at[hop, half],
            up,
        )

    def go_down(hop, half):
        copies.send(
            out_down.at[hop, span(half)],
            in_down.at[hop, span(half)],
            down_send.at[hop, half],
            down_recv.at[hop, half],
            down,
        )

    def from_up(hop, half):
        copies.arrived(
            in_up.at[hop, span(half)], up_send.at[hop, half], up_recv.at[hop, half], up
        )
        return in_up[hop, span(half), :].astype(F32)

    def from_down(hop, half):
        copies.arrived(
            in_down.at[hop, span(half)], down_send.at[hop, half], down_recv.at[hop, half], down
        )
        return in_down[hop, span(half), :].astype(F32)

    paired(4)
    out_up[0, span(0), :] = own(4, 0).astype(BF16)
    out_down[0, span(1), :] = own(-4, 1).astype(BF16)
    go_up(0, 0)
    go_down(0, 1)
    paired(3)
    paired(-3)
    out_up[1, span(1), :] = own(3, 1).astype(BF16)
    out_down[1, span(0), :] = own(-3, 0).astype(BF16)
    go_up(1, 1)
    go_down(1, 0)
    for hop in range(1, 4):
        d = 4 - hop
        if hop > 1:
            paired(d)
            paired(-d)
        out_up[hop, span(0), :] = (from_up(hop - 1, 0) + own(d, 0)).astype(BF16)
        out_down[hop, span(1), :] = (from_down(hop - 1, 1) + own(-d, 1)).astype(BF16)
        go_up(hop, 0)
        go_down(hop, 1)
        if hop > 1:
            out_up[hop, span(1), :] = (from_up(hop - 1, 1) + own(d, 1)).astype(BF16)
            out_down[hop, span(0), :] = (from_down(hop - 1, 0) + own(-d, 0)).astype(BF16)
            go_up(hop, 1)
            go_down(hop, 0)
    paired(0)
    for half in range(2):
        sums[span(half), :] = (
            own(0, half) + from_up(3, half) + from_down(3, half)
        ).astype(BF16)
    for o, (dy, dx) in enumerate(OFFSETS[:-1]):
        part = pl.ds(o * CAP, CAP)
        copies.send(
            sums.at[part],
            slots.at[part],
            back_send.at[o],
            back_recv.at[o],
            (sp_at(-dy, -dx), tp),
        )
    here = pl.ds((len(OFFSETS) - 1) * CAP, CAP)
    slots[here, :] = sums[here, :]
    at = lax.broadcasted_iota(jnp.int32, (tokens, rows), 1)
    chosen = ((row_ref[:, 0:1] == at) | (row_ref[:, 1:2] == at)).astype(BF16)
    fetch.wait()
    for o in range(len(OFFSETS) - 1):
        copies.arrived(slots.at[pl.ds(o * CAP, CAP)], back_send.at[o], back_recv.at[o], partner)
    total = jnp.dot(chosen, slots[...], preferred_element_type=F32)
    mixed[...] = (cot_buf[...].astype(F32) + total).astype(BF16)

    def block(g, c, half):
        return m_ref.at[
            pl.ds(half * half_tokens, half_tokens),
            pl.ds(pl.multiple_of((g * 2 + c) * 128, 128), 128),
        ]

    def spread(src, g, k, half, going_up, going_down, slot):
        dst = block(g, core, half)
        if going_up:
            copies.send(src, dst, gup_send.at[k, half], gup_recv.at[k, half], up)
        if going_down:
            copies.send(src, dst, gdown_send.at[k, half], gdown_recv.at[k, half], down)
        copies.send(src, dst, share_send.at[slot, half], share_recv.at[slot, half], partner)

    keep = []
    for half in range(2):
        src = mixed.at[pl.ds(half * half_tokens, half_tokens)]
        spread(src, z, 0, half, True, True, 0)
        copy = pltpu.make_async_copy(src, block(z, core, half), local_sem.at[1 + half])
        copy.start()
        keep.append(copy)
    for k in range(1, 5):
        above, below = (z + RING - k) % RING, (z + k) % RING
        for half in range(2):
            if k < 4 or half == 0:
                dst = block(above, core, half)
                copies.arrived(dst, gup_send.at[k - 1, half], gup_recv.at[k - 1, half], up)
                spread(dst, above, k, half, k < 3 or (k == 3 and half == 0), False, k)
            if k < 4 or half == 1:
                dst = block(below, core, half)
                copies.arrived(dst, gdown_send.at[k - 1, half], gdown_recv.at[k - 1, half], down)
                spread(
                    dst,
                    below,
                    k,
                    half,
                    False,
                    k < 3 or (k == 3 and half == 1),
                    4 if k == 4 else 4 + k,
                )
    for slot in range(RING):
        g = (z + RING - slot) % RING if slot <= 4 else (z + slot - 4) % RING
        for half in range(2):
            copies.arrived(
                block(g, 1 - core, half),
                share_send.at[slot, half],
                share_recv.at[slot, half],
                partner,
            )
    for copy in keep:
        copy.wait()
    copies.finish()


def collect(shares, rows_of, cotangent):
    dma = pltpu.SemaphoreType.DMA
    rows = shares.shape[2]
    tokens = cotangent.shape[0]
    n_back = len(OFFSETS) - 1
    vmem = pl.BlockSpec(memory_space=pltpu.VMEM)
    return pl.pallas_call(
        collect_kernel,
        out_shape=jax.ShapeDtypeStruct((tokens, D), BF16),
        in_specs=[vmem, vmem, pl.BlockSpec(memory_space=pl.ANY)],
        out_specs=vmem,
        scratch_shapes=[
            pltpu.VMEM((RING, rows, 128), BF16),
            pltpu.VMEM((4, rows, 128), BF16),
            pltpu.VMEM((4, rows, 128), BF16),
            pltpu.VMEM((4, rows, 128), BF16),
            pltpu.VMEM((4, rows, 128), BF16),
            pltpu.VMEM((rows, 128), BF16),
            pltpu.VMEM((rows, 128), BF16),
            pltpu.VMEM((tokens, 128), BF16),
            pltpu.VMEM((tokens, 128), BF16),
            dma((RING,)),
            dma((RING,)),
            dma((4, 2)),
            dma((4, 2)),
            dma((4, 2)),
            dma((4, 2)),
            dma((n_back,)),
            dma((n_back,)),
            dma((4, 2)),
            dma((4, 2)),
            dma((4, 2)),
            dma((4, 2)),
            dma((RING, 2)),
            dma((RING, 2)),
            dma((3,)),
        ],
        compiler_params=pltpu.CompilerParams(
            collective_id=1, has_side_effects=True, vmem_limit_bytes=32 << 20
        ),
        name="collect",
    )(shares, rows_of, cotangent)


def cut_along(value, dim, devices):
    before, after = (value.shape[:dim], value.shape[dim + 1 :])
    return jnp.moveaxis(value.reshape(*before, devices, -1, *after), dim, 0)


def sent_and_summed(value, axis, dim):
    devices = lax.axis_size(axis)
    tiles = lax.all_to_all(cut_along(value, dim, devices), axis, 0, 0, tiled=True)
    return jnp.sum(tiles.astype(F32), axis=0)


def of_everyone(value, axis):
    copies = jnp.broadcast_to(value, (lax.axis_size(axis), *value.shape))
    everything = lax.all_to_all(copies, axis, split_axis=0, concat_axis=0, tiled=True)
    return jnp.sum(everything, axis=0)


def from_behind(value, axis, by):
    devices = lax.axis_size(axis)
    pairs = [(i, i + by) for i in range(devices) if 0 <= i + by < devices]
    return lax.ppermute(value, axis, pairs)


def on_device(
    saved_input,
    cotangent,
    expert_ids,
    route_weight,
    w_gate,
    w_up,
    w_down,
    w_out,
    channel_gain,
    conv_taps,
    glu_value,
    glu_gate,
    conv_out,
    norm_mean,
    norm_rstd,
):
    tokens_here = cotangent.shape[0]
    gate_weight, up_weight, down_weight = w_gate[0], w_up[0], w_down[0]
    x, rows_of = select(expert_ids, route_weight, saved_input, cotangent)
    arrived = dispatch(x).reshape(2, len(OFFSETS) * CAP, D)
    rows_in, rows_cot = arrived[0], arrived[1]

    gate_pre = jnp.dot(rows_in, gate_weight, preferred_element_type=F32)
    up_pre = jnp.dot(rows_in, up_weight, preferred_element_type=F32)
    sigma = jax.nn.sigmoid(gate_pre)
    hidden = (gate_pre * sigma * up_pre).astype(BF16)
    hidden_cot = contract(rows_cot, down_weight, 1, 1)
    gate_cot = (hidden_cot * up_pre * sigma * (1.0 + gate_pre * (1.0 - sigma))).astype(BF16)
    up_cot = (hidden_cot * gate_pre * sigma).astype(BF16)
    shares = input_shares(gate_cot, up_cot, gate_weight, up_weight)
    mixed_cot = collect(shares, rows_of, cotangent)
    down_grad = contract(hidden, rows_cot, 0, 0).astype(BF16)[None]
    gate_grad = contract(rows_in, gate_cot, 0, 0).astype(BF16)[None]
    up_grad = contract(rows_in, up_cot, 0, 0).astype(BF16)[None]

    centered = (conv_out.astype(F32) - norm_mean[None, :]) * norm_rstd[None, :]
    normed = centered * channel_gain[:, None]
    sigma = jax.nn.sigmoid(normed)
    output_act = (normed * sigma).astype(BF16)
    proj_grad = sent_and_summed(contract(mixed_cot, output_act, 0, 1).astype(BF16), "sp", 0)
    act_cot = contract(w_out, mixed_cot, 0, 1)
    norm_cot = act_cot * sigma * (1.0 + normed * (1.0 - sigma)) * channel_gain[:, None]
    sums = of_everyone(
        jnp.stack([jnp.sum(norm_cot, axis=0), jnp.sum(norm_cot * centered, axis=0)]), "tp"
    )
    first_sum, second_sum = sums[0], sums[1]
    conv_cot = norm_rstd[None, :] * (
        norm_cot - first_sum[None, :] / C - centered * second_sum[None, :] / C
    )
    reach = conv_taps.shape[0] - 1
    rim = from_behind(conv_cot[:, :reach], "sp", -1)
    padded = jnp.concatenate([conv_cot, rim], axis=1)
    glu_cot = conv_taps[0][:, None] * padded[:, :tokens_here]
    for lag in range(1, reach + 1):
        glu_cot = glu_cot + conv_taps[lag][:, None] * padded[:, lag : lag + tokens_here]
    gate_sigma = jax.nn.sigmoid(glu_gate.astype(F32))
    value_grad = (glu_cot * gate_sigma).astype(BF16)
    gate_in_grad = (glu_cot * glu_value.astype(F32) * gate_sigma * (1.0 - gate_sigma)).astype(BF16)
    return (gate_grad, up_grad, down_grad, proj_grad, value_grad, gate_in_grad)


def solution(mesh):
    in_specs = (
        P("sp", None),
        P("sp", None),
        P("sp", None),
        P("sp", None),
        P("sp", None, "tp"),
        P("sp", None, "tp"),
        P("sp", "tp", None),
        P(None, "tp"),
        P("tp"),
        P(None, "tp"),
        P("tp", "sp"),
        P("tp", "sp"),
        P("tp", "sp"),
        P("sp"),
        P("sp"),
    )
    out_specs = (
        P("sp", None, "tp"),
        P("sp", None, "tp"),
        P("sp", "tp", None),
        P("sp", "tp"),
        P("tp", "sp"),
        P("tp", "sp"),
    )
    return jax.shard_map(
        on_device, mesh=mesh, in_specs=in_specs, out_specs=out_specs, check_vma=False
    )
```

time: 377 us -> 163 us (0.43)
  the two profiles are of different devices: /device:TPU:24 before, /device:TPU:1 now
where the time goes in v1:
time: 163 us
  Pallas kernels  105 us (64%)
  matrix products  28 us (17%)
  starting transfers between devices  10.5 us (6%)
  local copies, waits for them, and re-layouts  9.92 us (6%)
  waiting for transfers between devices  6.35 us (4%)
  other arithmetic  2.16 us (1%)
    pallas_call x1, Pallas kernels, collect(): pl.pallas_call(collect_kernel, out_shape=jax.ShapeDtypeStruct((tokens, D)...  53.2 us
    pallas_call x1, Pallas kernels, dispatch(): pl.pallas_call(dispatch_kernel, out_shape=jax.ShapeDtypeStruct((2, *x.sha...  41.1 us
    dot_general x6, matrix products, contract(): lax.dot_general(left, right, (((left_dim,), (right_dim,)), ((), ())), pre...  21 us
    unnamed x61, local copies, waits for them, and re-layouts  6.75 us
    pallas_call x1, Pallas kernels, input_shares(): pl.pallas_call(input_kernel, grid=(RING,), out_shape=jax.ShapeDtypeStruct...  6.09 us
    ppermute x1, waiting for transfers between devices, from_behind(): return lax.ppermute(value, axis, pairs)  5.32 us
    all_to_all x1, starting transfers between devices, of_everyone(): lax.all_to_all(copies, axis, split_axis=0, concat_axis=0, tiled=True)  4.72 us
    pallas_call x1, Pallas kernels, select(): pl.pallas_call(select_kernel, out_shape=(jax.ShapeDtypeStruct((len(OFFSET...  4.51 us
  transfers between devices with their start and end apart: 3, of which 2 were waited for; matrix products, arithmetic and copies ran while one was open for 11% of the time, Pallas kernels for 0%

profile of v1, /device:TPU:1, one launch (start us, length us, event | category | flops | bytes accessed | tf_op | source)
XLA Modules:
  0.0 162.8 jit_solution(4689024634920602736)
XLA Ops:
  0.6 0.0 copy-start
  0.6 0.9 copy.35.ids_ref
  1.6 0.8 copy.36.weight_ref
  2.4 0.0 copy-start.1
  2.4 1.2 copy-done.1
  3.6 1.2 copy-done.6
  4.9 4.5 %select.1 = (bf16[16,8,8,2048]{3,2,1,0:T(8,128)(2,1)S(1)}, s32[256,2]{1,0:T(8,128)S(1)}) custom-call(s32[256,2]{1,0:T(8,128)S(1)} %copy.35.ids_ref, f32[256,2]{1,0:T(8,128)S(1)} %copy.36.weight_ref, bf16[256,2048]{1,0:T(8,128)(2,1)S(1)} %copy-done.6, bf16[256,2048]{1,0:T(8,128)(2,1)S(1)} %copy-done.1), custom_call_target="tpu_custom_call" | custom-call | tf_op jit(solution)/shard_map/select/pallas_call | solution.py:130
  9.4 41.1 %dispatch.1 = bf16[2,16,8,8,2048]{4,3,2,1,0:T(8,128)(2,1)S(1)} custom-call(bf16[16,8,8,2048]{3,2,1,0:T(8,128)(2,1)S(1)} %get-tuple-element.8.x_ref), custom_call_target="tpu_custom_call" | custom-call | tf_op jit(solution)/shard_map/dispatch/pallas_call | solution.py:253
  50.5 0.0 copy-start.3
  50.5 2.5 %fusion.111 = (bf16[1,16,8,8,2048]{4,3,2,1,0:T(8,128)(2,1)}, bf16[1,16,8,8,2048]{4,3,2,1,0:T(8,128)(2,1)S(1)}) fusion(bf16[2,16,8,8,2048]{4,3,2,1,0:T(8,128)(2,1)S(1)} %dispatch.1), kind=kLoop, calls=%fused_computation.220 | loop fusion | bytes 16777216 | tf_op jit(solution)/shard_map/slice | solution.py:583
  53.0 0.0 copy-done.3
  53.0 3.5 %fusion.103 = f32[1024,384]{1,0:T(8,128)} fusion(bf16[1024,2048]{1,0:T(8,128)(2,1)S(1)} %bitcast.109, bf16[1,2048,384]{2,1,0:T(8,128)(2,1)S(1)} %copy-done.3), kind=kOutput, calls=%fused_computation.213 | convolution fusion | flops 1610612736 | bytes 7340032 | tf_op jit(solution)/shard_map/dot_general | solution.py:585
  56.5 0.0 copy-done.12
  56.5 0.0 copy-done.4
  56.5 3.5 %fusion.105 = f32[1024,384]{1,0:T(8,128)} fusion(bf16[1024,2048]{1,0:T(8,128)(2,1)S(1)} %bitcast.110, bf16[1,2048,384]{2,1,0:T(8,128)(2,1)S(1)} %copy-done.4), kind=kOutput, calls=%fused_computation.215 | convolution fusion | flops 1610612736 | bytes 7340032 | tf_op jit(solution)/shard_map/dot_general | solution.py:586
  60.0 0.0 copy-done.17
  60.0 0.7 copy.37
  60.8 0.0 copy-done
  60.8 6.0 %multiply_convert_fusion.1 = (bf16[1024,384]{1,0:T(8,128)(2,1)S(1)}, bf16[1024,384]{1,0:T(8,128)(2,1)S(1)}) fusion(f32[1024,384]{1,0:T(8,128)} %fusion.103, f32[1024,384]{1,0:T(8,128)} %fusion.105, bf16[1024,2048]{1,0:T(8,128)(2,1)} %bitcast.107, bf16[1,384,2048]{2,1,0:T(8,128)(2,1)S(1)} %copy-done), kind=kOutput, calls=%fused_computation.39 | convolution fusion | flops 1615724544 | bytes 10485760 | tf_op jit(solution)/shard_map/dot_general | solution.py:32
  66.7 0.0 copy-start.7
  66.8 0.0 copy-start.9
  66.8 0.0 copy-done.5
  66.8 0.0 copy-start.2
  66.8 6.1 %input_shares.1.p_ref = bf16[2,8,1024,128]{3,2,1,0:T(8,128)(2,1)S(1)} custom-call(bf16[1024,384]{1,0:T(8,128)(2,1)S(1)} %get-tuple-element.35.gate_ref, bf16[1024,384]{1,0:T(8,128)(2,1)S(1)} %get-tuple-element.34.up_ref, bf16[2048,384]{1,0:T(8,128)(2,1)S(1)} %bitcast.105, bf16[2048,384]{1,0:T(8,128)(2,1)S(1)} %bitcast.106), custom_call_target="tpu_custom_call" | custom-call | tf_op jit(solution)/shard_map/input_shares/pallas_call | solution.py:291
  72.9 0.0 copy-done.7
  72.9 0.0 copy-done.9
  72.9 0.0 copy-done.2
  72.9 0.0 copy-start.14
  72.9 0.0 copy-start.21
  72.9 0.0 copy-start.22
  73.0 0.0 copy-start.23
  73.0 0.0 copy-start.24
  73.0 53.2 %collect.1 = bf16[256,2048]{1,0:T(8,128)(2,1)S(1)} custom-call(bf16[2,8,1024,128]{3,2,1,0:T(8,128)(2,1)S(1)} %input_shares.1.p_ref, s32[256,2]{1,0:T(8,128)S(1)} %get-tuple-element.9.row_ref, bf16[256,2048]{1,0:T(8,128)(2,1)S(1)} %copy-done.2), custom_call_target="tpu_custom_call" | custom-call | tf_op jit(solution)/shard_map/collect/pallas_call | solution.py:501
  126.1 0.0 copy-done.14
  126.2 0.0 copy-done.21
  126.2 0.0 copy-done.22
  126.2 0.0 copy-done.23
  126.2 0.0 copy-done.24
  126.2 0.0 copy-start.10
  126.2 1.1 fusion.109
  127.3 0.6 broadcast_in_dim.20
  127.9 4.7 %all-to-all-start.1 = ((f32[16,2,256]{2,1,0:T(2,128)}), f32[16,2,256]{2,1,0:T(2,128)}, u32[]{:S(2)}, u32[]{:S(2)}) async-start(f32[16,2,256]{2,1,0:T(2,128)} %broadcast_in_dim.20), calls=%async_computation.1 | async-start | bytes 65536 | tf_op jit(solution)/shard_map/all_to_all | solution.py:552
  132.7 0.0 copy-done.10
  132.7 5.9 %fusion = bf16[1,2048,384]{2,1,0:T(8,128)(2,1)} fusion(bf16[1024,2048]{1,0:T(8,128)(2,1)} %bitcast.111, bf16[1024,384]{1,0:T(8,128)(2,1)S(1)} %copy-done.10), kind=kOutput, calls=%fused_computation.3 | convolution fusion | flops 1611399168 | bytes 6553600 | tf_op jit(solution)/shard_map/dot_general | solution.py:32
  138.5 0.0 copy-done.8
  138.6 3.6 %fusion.1 = bf16[1,2048,384]{2,1,0:T(8,128)(2,1)} fusion(bf16[1024,2048]{1,0:T(8,128)(2,1)S(1)} %bitcast.112, bf16[1024,384]{1,0:T(8,128)(2,1)S(1)} %copy-done.8), kind=kOutput, calls=%fused_computation.4 | convolution fusion | flops 1611399168 | bytes 6553600 | tf_op jit(solution)/shard_map/dot_general | solution.py:32
  142.2 3.1 %fusion.2 = bf16[1,384,2048]{2,1,0:T(8,128)(2,1)} fusion(bf16[1024,2048]{1,0:T(8,128)(2,1)S(1)} %bitcast.108, f32[1024,384]{1,0:T(8,128)S(1)} %copy-done.26, f32[1024,384]{1,0:T(8,128)S(1)} %copy-done.25), kind=kOutput, calls=%fused_computation.5 | convolution fusion | flops 1613758464 | bytes 8912896 | tf_op jit(solution)/shard_map/dot_general | solution.py:32
  145.3 0.0 copy-start.19
  145.3 1.4 convolution_convert_fusion.3
  146.7 0.0 all-to-all-done.1
  146.7 4.5 %all-to-all-start = ((bf16[16,128,128]{2,1,0:T(8,128)(2,1)}), bf16[16,128,128]{2,1,0:T(8,128)(2,1)S(1)}, u32[]{:S(2)}, u32[]{:S(2)}) async-start(bf16[16,128,128]{2,1,0:T(8,128)(2,1)} %bitcast.8), calls=%async_computation | async-start | bytes 1048576 | tf_op jit(solution)/shard_map/all_to_all | solution.py:546
  151.2 0.8 reduce_sum.39
  152.0 0.0 copy-done.16
  152.0 0.2 subtract_multiply_fusion
  152.3 1.3 collective-permute-start
  153.6 0.1 copy.40
  153.7 0.0 copy-done.19
  153.7 0.1 copy.39
  153.8 5.3 %collective-permute-done = f32[128,30]{0,1:T(8,128)S(1)} collective-permute-done((f32[128,30]{0,1:T(8,128)S(1)}, f32[128,30]{0,1:T(8,128)S(1)}, u32[]{:S(2)}, u32[]{:S(2)}) %collective-permute-start) | collective-permute-done | bytes 15392 | tf_op jit(solution)/shard_map/ppermute | solution.py:559
  159.2 0.4 multiply_convert_fusion.4
  159.6 0.7 copy.41
  160.4 0.7 copy.42
  161.1 1.0 all-to-all-done
  162.1 0.7 convert_reduce_fusion
  (27 shorter events, 0.1 us)
Async XLA Ops:
  0.6 60.1 %copy-start = (bf16[1,384,2048]{2,1,0:T(8,128)(2,1)S(1)}, bf16[1,384,2048]{2,1,0:T(8,128)(2,1)}, u32[]{:S(2)}) copy-start(bf16[1,384,2048]{2,1,0:T(8,128)(2,1)} %param.21) | copy-start | bytes 4718596
  2.4 1.2 copy-start.1
  3.6 1.2 copy-start.6
  50.5 2.5 %copy-start.3 = (bf16[1,2048,384]{2,1,0:T(8,128)(2,1)S(1)}, bf16[1,2048,384]{2,1,0:T(8,128)(2,1)}, u32[]{:S(2)}) copy-start(bf16[1,2048,384]{2,1,0:T(8,128)(2,1)} %param.19) | copy-start | bytes 4718596
  53.0 3.5 %copy-start.12 = (bf16[1,16,8,8,2048]{4,3,2,1,0:T(8,128)(2,1)}, bf16[1,16,8,8,2048]{4,3,2,1,0:T(8,128)(2,1)S(1)}, u32[]{:S(2)}) copy-start(bf16[1,16,8,8,2048]{4,3,2,1,0:T(8,128)(2,1)S(1)} %get-tuple-element.33) | copy-start | bytes 12582916
  53.0 3.5 %copy-start.4 = (bf16[1,2048,384]{2,1,0:T(8,128)(2,1)S(1)}, bf16[1,2048,384]{2,1,0:T(8,128)(2,1)}, u32[]{:S(2)}) copy-start(bf16[1,2048,384]{2,1,0:T(8,128)(2,1)} %param.20) | copy-start | bytes 4718596
  56.5 3.5 %copy-start.17 = (bf16[128,256]{1,0:T(8,128)(2,1)S(1)}, bf16[128,256]{1,0:T(8,128)(2,1)}, u32[]{:S(2)}) copy-start(bf16[128,256]{1,0:T(8,128)(2,1)} %param.27) | copy-start | bytes 196612
  60.8 6.0 %copy-start.5 = (bf16[1,2048,384]{2,1,0:T(8,128)(2,1)S(1)}, bf16[1,2048,384]{2,1,0:T(8,128)(2,1)}, u32[]{:S(2)}) copy-start(bf16[1,2048,384]{2,1,0:T(8,128)(2,1)} %param.20) | copy-start | bytes 4718596
  66.7 6.1 %copy-start.7 = (bf16[1024,384]{1,0:T(8,128)(2,1)}, bf16[1024,384]{1,0:T(8,128)(2,1)S(1)}, u32[]{:S(2)}) copy-start(bf16[1024,384]{1,0:T(8,128)(2,1)S(1)} %get-tuple-element.34.up_ref) | copy-start | bytes 2359300
  66.8 6.1 %copy-start.9 = (bf16[1024,384]{1,0:T(8,128)(2,1)}, bf16[1024,384]{1,0:T(8,128)(2,1)S(1)}, u32[]{:S(2)}) copy-start(bf16[1024,384]{1,0:T(8,128)(2,1)S(1)} %get-tuple-element.35.gate_ref) | copy-start | bytes 2359300
  66.8 6.1 %copy-start.2 = (bf16[256,2048]{1,0:T(8,128)(2,1)S(1)}, bf16[256,2048]{1,0:T(8,128)(2,1)}, u32[]{:S(2)}) copy-start(bf16[256,2048]{1,0:T(8,128)(2,1)} %cot_ref.3) | copy-start | bytes 3145732
  72.9 53.2 %copy-start.14 = (bf16[128,256]{0,1:T(8,128)(2,1)S(1)}, bf16[128,256]{0,1:T(8,128)(2,1)}, u32[]{:S(2)}) copy-start(bf16[128,256]{0,1:T(8,128)(2,1)} %copy.37) | copy-start | bytes 196612
  72.9 53.2 %copy-start.21 = (f32[256]{0:T(256)S(1)}, f32[256]{0:T(256)}, u32[]{:S(2)}) copy-start(f32[256]{0:T(256)} %param.29) | copy-start | bytes 3076
  72.9 53.2 %copy-start.22 = (f32[256]{0:T(256)S(1)}, f32[256]{0:T(256)}, u32[]{:S(2)}) copy-start(f32[256]{0:T(256)} %param.28) | copy-start | bytes 3076
  73.0 53.2 %copy-start.23 = (bf16[2048,128]{1,0:T(8,128)(2,1)S(1)}, bf16[2048,128]{1,0:T(8,128)(2,1)}, u32[]{:S(2)}) copy-start(bf16[2048,128]{1,0:T(8,128)(2,1)} %param.22) | copy-start | bytes 1572868
  73.0 53.2 %copy-start.24 = (f32[128]{0:T(128)S(1)}, f32[128]{0:T(128)}, u32[]{:S(2)}) copy-start(f32[128]{0:T(128)} %param.23) | copy-start | bytes 1540
  126.2 6.5 %copy-start.10 = (bf16[1024,384]{1,0:T(8,128)(2,1)S(1)}, bf16[1024,384]{1,0:T(8,128)(2,1)}, u32[]{:S(2)}) copy-start(bf16[1024,384]{1,0:T(8,128)(2,1)} %copy-done.9) | copy-start | bytes 2359300
  127.9 18.8 %all-to-all-start.1 = ((f32[16,2,256]{2,1,0:T(2,128)}), f32[16,2,256]{2,1,0:T(2,128)}, u32[]{:S(2)}, u32[]{:S(2)}) async-start(f32[16,2,256]{2,1,0:T(2,128)} %broadcast_in_dim.20), calls=%async_computation.1 | async-start | bytes 65536 | tf_op jit(solution)/shard_map/all_to_all | solution.py:552
  132.7 5.9 %copy-start.8 = (bf16[1024,384]{1,0:T(8,128)(2,1)S(1)}, bf16[1024,384]{1,0:T(8,128)(2,1)}, u32[]{:S(2)}) copy-start(bf16[1024,384]{1,0:T(8,128)(2,1)} %copy-done.7) | copy-start | bytes 2359300
  132.7 5.9 %copy-start.13 = (bf16[1,16,8,8,2048]{4,3,2,1,0:T(8,128)(2,1)S(1)}, bf16[1,16,8,8,2048]{4,3,2,1,0:T(8,128)(2,1)}, u32[]{:S(2)}) copy-start(bf16[1,16,8,8,2048]{4,3,2,1,0:T(8,128)(2,1)} %copy-done.12) | copy-start | bytes 12582916
  138.6 3.6 %copy-start.11 = (bf16[1,16,8,8,2048]{4,3,2,1,0:T(8,128)(2,1)S(1)}, bf16[1,16,8,8,2048]{4,3,2,1,0:T(8,128)(2,1)}, u32[]{:S(2)}) copy-start(bf16[1,16,8,8,2048]{4,3,2,1,0:T(8,128)(2,1)} %get-tuple-element.32) | copy-start | bytes 12582916
  138.6 3.6 %copy-start.25 = (f32[1024,384]{1,0:T(8,128)S(1)}, f32[1024,384]{1,0:T(8,128)}, u32[]{:S(2)}) copy-start(f32[1024,384]{1,0:T(8,128)} %fusion.103) | copy-start | bytes 4718596
  138.6 3.6 %copy-start.26 = (f32[1024,384]{1,0:T(8,128)S(1)}, f32[1024,384]{1,0:T(8,128)}, u32[]{:S(2)}) copy-start(f32[1024,384]{1,0:T(8,128)} %fusion.105) | copy-start | bytes 4718596
  142.2 3.1 %copy-start.15 = (bf16[128,256]{0,1:T(8,128)(2,1)S(1)}, bf16[128,256]{0,1:T(8,128)(2,1)}, u32[]{:S(2)}) copy-start(bf16[128,256]{0,1:T(8,128)(2,1)} %copy.37) | copy-start | bytes 196612
  145.3 1.4 copy-start.20
  145.3 6.7 %copy-start.16 = (f32[128,256]{0,1:T(8,128)S(1)}, f32[128,256]{0,1:T(8,128)}, u32[]{:S(2)}) copy-start(f32[128,256]{0,1:T(8,128)} %get-tuple-element.69) | copy-start | bytes 393220
  145.3 8.3 %copy-start.18 = (bf16[128,256]{1,0:T(8,128)(2,1)S(1)}, bf16[128,256]{1,0:T(8,128)(2,1)}, u32[]{:S(2)}) copy-start(bf16[128,256]{1,0:T(8,128)(2,1)} %param.25) | copy-start | bytes 196612
  145.3 8.4 %copy-start.19 = (bf16[128,256]{1,0:T(8,128)(2,1)S(1)}, bf16[128,256]{1,0:T(8,128)(2,1)}, u32[]{:S(2)}) copy-start(bf16[128,256]{1,0:T(8,128)(2,1)} %param.26) | copy-start | bytes 196612
  146.7 15.4 %all-to-all-start = ((bf16[16,128,128]{2,1,0:T(8,128)(2,1)}), bf16[16,128,128]{2,1,0:T(8,128)(2,1)S(1)}, u32[]{:S(2)}, u32[]{:S(2)}) async-start(bf16[16,128,128]{2,1,0:T(8,128)(2,1)} %bitcast.8), calls=%async_computation | async-start | bytes 1048576 | tf_op jit(solution)/shard_map/all_to_all | solution.py:546
  152.3 6.9 %collective-permute-start = (f32[128,30]{0,1:T(8,128)S(1)}, f32[128,30]{0,1:T(8,128)S(1)}, u32[]{:S(2)}, u32[]{:S(2)}) collective-permute-start(f32[128,30]{0,1:T(8,128)S(1)} %slice.268), channel_id=1, source_target_pairs={{16,0},{32,16},{48,32},{64,48},{80,64},{96,80},{112,96},{128,112},... | collective-permute-start | bytes 46088 | tf_op jit(solution)/shard_map/ppermute | solution.py:559

commit v2 on v0

v2 whole, which is shorter than its diff:
```python
import jax
import jax.numpy as jnp
from jax import lax
from jax.experimental import pallas as pl
from jax.experimental.pallas import tpu as pltpu
from jax.sharding import PartitionSpec as P

D = 2048
C = 2048
HIDDEN = 384
SIDE = 4
RING = 8
CAP = 64
BF16 = jnp.bfloat16
F32 = jnp.float32
MESH = pl.DeviceIdType.MESH

NEXT = ((0, 1), (0, 3), (1, 0), (3, 0))
CORNER = ((1, 1), (3, 3), (1, 3), (3, 1))
HERE = ((0, 0),)
ACROSS = ((0, 2), (2, 0))
FAR = ((1, 2), (3, 2), (2, 1), (2, 3), (2, 2))
OFFSETS = NEXT + CORNER + HERE + ACROSS + FAR
N_OFF = len(OFFSETS)
LOCAL = OFFSETS.index((0, 0))
FAR_AT = N_OFF - len(FAR)
HALVES = ((0, 3), (3, 2))
ROWS = N_OFF * CAP


def sp_at(dy, dx):
    sp = lax.axis_index("sp")
    y, x = sp // SIDE, sp % SIDE
    return ((y + dy) % SIDE) * SIDE + (x + dx) % SIDE


def contract(left, right, left_dim, right_dim):
    return lax.dot_general(
        left, right, (((left_dim,), (right_dim,)), ((), ())), preferred_element_type=F32
    )


class Copies:
    def __init__(self):
        self.started = []

    def send(self, src, dst, sems, at, device):
        copy = pltpu.make_async_remote_copy(
            src_ref=src,
            dst_ref=dst,
            send_sem=sems[0].at[at],
            recv_sem=sems[1].at[at],
            device_id=device,
            device_id_type=MESH,
        )
        copy.start()
        self.started.append(copy)

    def arrived(self, dst, sems, at, device):
        pltpu.make_async_remote_copy(
            src_ref=dst,
            dst_ref=dst,
            send_sem=sems[0].at[at],
            recv_sem=sems[1].at[at],
            device_id=device,
            device_id_type=MESH,
        ).wait_recv()

    def finish(self):
        for copy in self.started:
            copy.wait_send()


def spread_ring(copies, block, source, core, z, up, down, partner, ups, downs, shares, between):
    def spread(src, g, k, half, going_up, going_down, slot):
        dst = block(g, core, half)
        if going_up:
            copies.send(src, dst, ups, (k, half), up)
        if going_down:
            copies.send(src, dst, downs, (k, half), down)
        copies.send(src, dst, shares, (slot, half), partner)

    for half in range(2):
        spread(source(half), z, 0, half, True, True, 0)
    between(0)
    for k in range(1, 5):
        above, below = (z + RING - k) % RING, (z + k) % RING
        for half in range(2):
            if k < 4 or half == 0:
                here = block(above, core, half)
                copies.arrived(here, ups, (k - 1, half), up)
                spread(here, above, k, half, k < 3 or (k == 3 and half == 0), False, k)
            if k < 4 or half == 1:
                here = block(below, core, half)
                copies.arrived(here, downs, (k - 1, half), down)
                spread(
                    here,
                    below,
                    k,
                    half,
                    False,
                    k < 3 or (k == 3 and half == 1),
                    4 if k == 4 else 4 + k,
                )
        between(k)
    for slot in range(RING):
        g = (z + RING - slot) % RING if slot <= 4 else (z + slot - 4) % RING
        for half in range(2):
            copies.arrived(block(g, 1 - core, half), shares, (slot, half), partner)


def experts_kernel(
    ids_ref,
    weight_ref,
    in_ref,
    cot_ref,
    wg_ref,
    wu_ref,
    wd_ref,
    gg_ref,
    ug_ref,
    dg_ref,
    m_ref,
    src0,
    src1,
    x_far,
    x_near,
    r,
    wgu,
    wd,
    gu,
    hid,
    hid_t,
    p,
    pair_buf,
    out_up,
    in_up,
    out_down,
    in_down,
    sums,
    slots,
    chosen,
    mixed,
    *sems,
):
    (load_sem, *pairs) = sems
    (far_s, near_s, nshare_s, up_s, down_s, share_s, pair_s) = [
        (pairs[2 * i], pairs[2 * i + 1]) for i in range(7)
    ]
    (rup_s, rdown_s, back_s, gup_s, gdown_s, gshare_s) = [
        (pairs[2 * i], pairs[2 * i + 1]) for i in range(7, 13)
    ]
    sp, tp = lax.axis_index("sp"), lax.axis_index("tp")
    y, x = sp // SIDE, sp % SIDE
    z, core = tp // 2, tp % 2
    partner = (sp, z * 2 + 1 - core)
    up = (sp, ((z + 1) % RING) * 2 + core)
    down = (sp, ((z + RING - 1) % RING) * 2 + core)
    others = [partner, up, down]
    others += [(sp_at(dy, dx), tp) for dy, dx in OFFSETS if (dy, dx) != (0, 0)]
    barrier = pltpu.get_barrier_semaphore()
    for device in others:
        pl.semaphore_signal(barrier, inc=1, device_id=device, device_id_type=MESH)
    copies = Copies()
    tokens = in_ref.shape[0]

    loads = [
        pltpu.make_async_copy(wg_ref, wgu.at[:, pl.ds(0, HIDDEN)], load_sem.at[0]),
        pltpu.make_async_copy(wu_ref, wgu.at[:, pl.ds(HIDDEN, HIDDEN)], load_sem.at[1]),
        pltpu.make_async_copy(wd_ref, wd, load_sem.at[2]),
    ]
    for load in loads:
        load.start()

    n_experts = N_OFF
    expert = lax.broadcasted_iota(jnp.int32, (n_experts, tokens), 0)
    one = [(ids_ref[k : k + 1, :] == expert).astype(F32) for k in range(2)]
    earlier = (
        lax.broadcasted_iota(jnp.int32, (tokens, tokens), 0)
        < lax.broadcasted_iota(jnp.int32, (tokens, tokens), 1)
    ).astype(BF16)
    before = jnp.dot((one[0] + one[1]).astype(BF16), earlier, preferred_element_type=F32)
    place = jnp.zeros((n_experts, tokens), jnp.int32)
    for o, (dy, dx) in enumerate(OFFSETS):
        place = jnp.where(
            expert == ((y + dy) % SIDE) * SIDE + (x + dx) % SIDE, o * CAP, place
        )
    row_of = before + place.astype(F32)
    row_f = [jnp.sum(one[k] * row_of, axis=0, keepdims=True) for k in range(2)]
    row = [value.astype(jnp.int32) for value in row_f]

    def column(value):
        return jnp.transpose(jnp.broadcast_to(value, (128, tokens)))

    for k, src in enumerate((src0, src1)):
        scale = column(weight_ref[k : k + 1, :])
        for j in range(D // 128):
            part = pl.ds(j * 128, 128)
            scaled = (scale * cot_ref[:, part].astype(F32)).astype(BF16)
            src[:, part] = jnp.where(core == 0, in_ref[:, part], scaled)

    def picked(at):
        return (
            jnp.dot((row[0] == at).astype(BF16), src0[...], preferred_element_type=F32)
            + jnp.dot((row[1] == at).astype(BF16), src1[...], preferred_element_type=F32)
        ).astype(BF16)

    def fill(first, count):
        at = lax.broadcasted_iota(jnp.int32, (count * CAP, tokens), 0) + first * CAP
        x_near[pl.ds(first, count)] = picked(at).reshape(count, RING, 8, D)

    def send_near(first, count):
        for o in range(first, first + count):
            if o == LOCAL:
                copies.send(x_near.at[o], r.at[core, o], nshare_s, o, partner)
            else:
                copies.send(
                    x_near.at[o], r.at[core, o], near_s, o, (sp_at(*OFFSETS[o]), tp)
                )

    index = lax.broadcasted_iota(jnp.int32, (len(FAR) * 8, tokens), 0)
    x_far[...] = picked((FAR_AT + index // 8) * CAP + z * 8 + index % 8).reshape(len(FAR), 8, D)
    fill(0, 4)
    pl.semaphore_wait(barrier, len(others))
    for i, offset in enumerate(FAR):
        copies.send(
            x_far.at[i], r.at[core, FAR_AT + i, z], far_s, i, (sp_at(*offset), tp)
        )
    fill(4, 4)
    send_near(0, 4)
    fill(8, 3)
    send_near(4, 4)
    send_near(8, 3)
    r[core, LOCAL] = x_near[LOCAL]

    def far(g, c, half):
        start, size = HALVES[half]
        return r.at[c, pl.ds(FAR_AT + start, size), g]

    def forward(first, count):
        for o in range(first, first + count):
            if o != LOCAL:
                copies.arrived(r.at[core, o], near_s, o, partner)
                copies.send(r.at[core, o], r.at[core, o], nshare_s, o, partner)

    def shared(first, count):
        for o in range(first, first + count):
            copies.arrived(r.at[1 - core, o], nshare_s, o, partner)

    def forward_group(first, count):
        span = pl.ds(first * CAP, count * CAP)
        rows_in = r[0, pl.ds(first, count)].reshape(count * CAP, D)
        rows_cot = r[1, pl.ds(first, count)].reshape(count * CAP, D)
        both = jnp.dot(rows_in, wgu[...], preferred_element_type=F32)
        gate_pre, up_pre = both[:, :HIDDEN], both[:, HIDDEN:]
        hidden_cot = contract(rows_cot, wd[...], 1, 1)
        sigma = jax.nn.sigmoid(gate_pre)
        hid[span, :] = (gate_pre * sigma * up_pre).astype(BF16)
        gu[span, pl.ds(0, HIDDEN)] = (
            hidden_cot * up_pre * sigma * (1.0 + gate_pre * (1.0 - sigma))
        ).astype(BF16)
        gu[span, pl.ds(HIDDEN, HIDDEN)] = (hidden_cot * gate_pre * sigma).astype(BF16)

    def between(k):
        if k == 0:
            forward(0, 4)
            for load in loads:
                load.wait()
            shared(0, 4)
            forward_group(0, 4)
        if k == 2:
            forward(4, 5)
        if k == 3:
            shared(4, 5)
            forward_group(4, 5)
        if k == 4:
            forward(9, 2)
            shared(9, 2)
            forward_group(9, 2)

    for i in range(len(FAR)):
        copies.arrived(r.at[core, FAR_AT + i, z], far_s, i, partner)
    spread_ring(
        copies,
        far,
        lambda half: far(z, core, half),
        core,
        z,
        up,
        down,
        partner,
        up_s,
        down_s,
        share_s,
        between,
    )
    forward_group(FAR_AT, len(FAR))

    half_rows = ROWS // 2

    def at_z(d):
        return (z + RING + d) % RING

    def chunk(d):
        g = at_z(d)
        total = contract(
            gu[...], wgu[pl.ds(pl.multiple_of(g * 256, 256), 256), :], 1, 1
        ).astype(BF16)
        p[0, g] = total[:, :128]
        p[1, g] = total[:, 128:]
        copies.send(p.at[1 - core, g], pair_buf.at[g], pair_s, d % RING, partner)

    def paired(d):
        copies.arrived(pair_buf.at[at_z(d)], pair_s, d % RING, partner)

    def span(half):
        return pl.ds(half * half_rows, half_rows)

    def own(d, half):
        g = at_z(d)
        return p[core, g, span(half), :].astype(F32) + pair_buf[g, span(half), :].astype(F32)

    def go(hop, half_up, half_down):
        copies.send(
            out_up.at[hop, span(half_up)], in_up.at[hop, span(half_up)], rup_s, (hop, half_up), up
        )
        copies.send(
            out_down.at[hop, span(half_down)],
            in_down.at[hop, span(half_down)],
            rdown_s,
            (hop, half_down),
            down,
        )

    def came(buf, sem, hop, half):
        copies.arrived(buf.at[hop, span(half)], sem, (hop, half), partner)
        return buf[hop, span(half), :].astype(F32)

    def weight_grads(i):
        part = pl.ds(i * 256, 256)
        rows_in = r[0, :, :, :, part].reshape(ROWS, 256)
        rows_cot = r[1, :, :, :, part].reshape(ROWS, 256)
        both = contract(rows_in, gu[...], 0, 0).astype(BF16)
        gg_ref[part, :] = both[:, :HIDDEN]
        ug_ref[part, :] = both[:, HIDDEN:]
        dg_ref[:, part] = jnp.dot(hid_t[...], rows_cot, preferred_element_type=F32).astype(BF16)

    chunk(4)
    chunk(3)
    paired(4)
    out_up[0, span(0), :] = own(4, 0).astype(BF16)
    out_down[0, span(1), :] = own(-4, 1).astype(BF16)
    go(0, 0, 1)
    chunk(-3)
    paired(3)
    paired(-3)
    out_up[1, span(1), :] = own(3, 1).astype(BF16)
    out_down[1, span(0), :] = own(-3, 0).astype(BF16)
    go(1, 1, 0)
    chunk(2)
    chunk(-2)
    for hop in range(1, 4):
        d = 4 - hop
        if hop > 1:
            paired(d)
            paired(-d)
        out_up[hop, span(0), :] = (came(in_up, rup_s, hop - 1, 0) + own(d, 0)).astype(BF16)
        out_down[hop, span(1), :] = (came(in_down, rdown_s, hop - 1, 1) + own(-d, 1)).astype(BF16)
        go(hop, 0, 1)
        if hop == 1:
            chunk(1)
            chunk(-1)
        if hop > 1:
            out_up[hop, span(1), :] = (came(in_up, rup_s, hop - 1, 1) + own(d, 1)).astype(BF16)
            out_down[hop, span(0), :] = (came(in_down, rdown_s, hop - 1, 0) + own(-d, 0)).astype(
                BF16
            )
            go(hop, 1, 0)
        if hop == 2:
            chunk(0)
            hid_t[...] = jnp.transpose(hid[...])
            weight_grads(0)
        if hop == 3:
            weight_grads(1)
            weight_grads(2)
    paired(0)
    for half in range(2):
        sums[span(half), :] = (
            own(0, half) + came(in_up, rup_s, 3, half) + came(in_down, rdown_s, 3, half)
        ).astype(BF16)
    for o in reversed(range(N_OFF)):
        if o != LOCAL:
            dy, dx = OFFSETS[o]
            part = pl.ds(o * CAP, CAP)
            copies.send(sums.at[part], slots.at[part], back_s, o, (sp_at(-dy, -dx), tp))
    here = pl.ds(LOCAL * CAP, CAP)
    slots[here, :] = sums[here, :]
    where = [column(value).astype(jnp.int32) for value in row_f]
    for j in range(ROWS // 128):
        at = lax.broadcasted_iota(jnp.int32, (tokens, 128), 1) + j * 128
        chosen[:, pl.ds(j * 128, 128)] = ((where[0] == at) | (where[1] == at)).astype(BF16)
    weight_grads(3)
    weight_grads(4)
    for o in range(N_OFF):
        if o != LOCAL:
            copies.arrived(slots.at[pl.ds(o * CAP, CAP)], back_s, o, partner)
    total = jnp.dot(chosen[...], slots[...], preferred_element_type=F32)
    mine = pl.ds(pl.multiple_of(tp * 128, 128), 128)
    mixed[...] = (cot_ref[:, mine].astype(F32) + total).astype(BF16)

    half_tokens = tokens // 2

    def block(g, c, half):
        return m_ref.at[
            pl.ds(half * half_tokens, half_tokens),
            pl.ds(pl.multiple_of((g * 2 + c) * 128, 128), 128),
        ]

    def between_gather(k):
        if k == 0:
            m_ref[:, mine] = mixed[...]
            weight_grads(5)
        if k == 1:
            weight_grads(6)
        if k == 2:
            weight_grads(7)

    spread_ring(
        copies,
        block,
        lambda half: mixed.at[pl.ds(half * half_tokens, half_tokens)],
        core,
        z,
        up,
        down,
        partner,
        gup_s,
        gdown_s,
        gshare_s,
        between_gather,
    )
    copies.finish()


def experts(ids, weight, rows_in, cotangent, w_gate, w_up, w_down):
    dma = pltpu.SemaphoreType.DMA
    tokens = cotangent.shape[0]
    vmem = pl.BlockSpec(memory_space=pltpu.VMEM)
    anywhere = pl.BlockSpec(memory_space=pl.ANY)

    def both(*shape):
        return [dma(shape), dma(shape)]

    def buf(*shape):
        return pltpu.VMEM(shape, BF16)

    return pl.pallas_call(
        experts_kernel,
        out_shape=(
            jax.ShapeDtypeStruct((D, HIDDEN), BF16),
            jax.ShapeDtypeStruct((D, HIDDEN), BF16),
            jax.ShapeDtypeStruct((HIDDEN, D), BF16),
            jax.ShapeDtypeStruct((tokens, D), BF16),
        ),
        in_specs=[vmem] * 4 + [anywhere] * 3,
        out_specs=(vmem,) * 4,
        scratch_shapes=[
            buf(tokens, D),
            buf(tokens, D),
            buf(len(FAR), 8, D),
            buf(FAR_AT, RING, 8, D),
            buf(2, N_OFF, RING, 8, D),
            buf(D, 2 * HIDDEN),
            buf(HIDDEN, D),
            buf(ROWS, 2 * HIDDEN),
            buf(ROWS, HIDDEN),
            buf(HIDDEN, ROWS),
            buf(2, RING, ROWS, 128),
            buf(RING, ROWS, 128),
            buf(4, ROWS, 128),
            buf(4, ROWS, 128),
            buf(4, ROWS, 128),
            buf(4, ROWS, 128),
            buf(ROWS, 128),
            buf(ROWS, 128),
            buf(tokens, ROWS),
            buf(tokens, 128),
            dma((3,)),
            *both(len(FAR)),
            *both(FAR_AT),
            *both(FAR_AT),
            *both(4, 2),
            *both(4, 2),
            *both(RING, 2),
            *both(RING),
            *both(4, 2),
            *both(4, 2),
            *both(N_OFF),
            *both(4, 2),
            *both(4, 2),
            *both(RING, 2),
        ],
        compiler_params=pltpu.CompilerParams(
            collective_id=0, has_side_effects=True, vmem_limit_bytes=60 << 20
        ),
        name="experts",
    )(ids, weight, rows_in, cotangent, w_gate, w_up, w_down)


def cut_along(value, dim, devices):
    before, after = (value.shape[:dim], value.shape[dim + 1 :])
    return jnp.moveaxis(value.reshape(*before, devices, -1, *after), dim, 0)


def sent_and_summed(value, axis, dim):
    devices = lax.axis_size(axis)
    tiles = lax.all_to_all(cut_along(value, dim, devices), axis, 0, 0, tiled=True)
    return jnp.sum(tiles.astype(F32), axis=0)


def of_everyone(value, axis):
    copies = jnp.broadcast_to(value, (lax.axis_size(axis), *value.shape))
    everything = lax.all_to_all(copies, axis, split_axis=0, concat_axis=0, tiled=True)
    return jnp.sum(everything, axis=0)


def from_behind(value, axis, by):
    devices = lax.axis_size(axis)
    pairs = [(i, i + by) for i in range(devices) if 0 <= i + by < devices]
    return lax.ppermute(value, axis, pairs)


def on_device(
    saved_input,
    cotangent,
    expert_ids,
    route_weight,
    w_gate,
    w_up,
    w_down,
    w_out,
    channel_gain,
    conv_taps,
    glu_value,
    glu_gate,
    conv_out,
    norm_mean,
    norm_rstd,
):
    tokens_here = cotangent.shape[0]
    gate_grad, up_grad, down_grad, mixed_cot = experts(
        expert_ids.T, route_weight.T, saved_input, cotangent, w_gate[0], w_up[0], w_down[0]
    )

    centered = (conv_out.astype(F32) - norm_mean[None, :]) * norm_rstd[None, :]
    normed = centered * channel_gain[:, None]
    sigma = jax.nn.sigmoid(normed)
    output_act = (normed * sigma).astype(BF16)
    proj_grad = sent_and_summed(contract(mixed_cot, output_act, 0, 1).astype(BF16), "sp", 0)
    act_cot = contract(w_out, mixed_cot, 0, 1)
    norm_cot = act_cot * sigma * (1.0 + normed * (1.0 - sigma)) * channel_gain[:, None]
    sums = of_everyone(
        jnp.stack([jnp.sum(norm_cot, axis=0), jnp.sum(norm_cot * centered, axis=0)]), "tp"
    )
    first_sum, second_sum = sums[0], sums[1]
    conv_cot = norm_rstd[None, :] * (
        norm_cot - first_sum[None, :] / C - centered * second_sum[None, :] / C
    )
    reach = conv_taps.shape[0] - 1
    rim = from_behind(conv_cot[:, :reach], "sp", -1)
    padded = jnp.concatenate([conv_cot, rim], axis=1)
    glu_cot = conv_taps[0][:, None] * padded[:, :tokens_here]
    for lag in range(1, reach + 1):
        glu_cot = glu_cot + conv_taps[lag][:, None] * padded[:, lag : lag + tokens_here]
    gate_sigma = jax.nn.sigmoid(glu_gate.astype(F32))
    value_grad = (glu_cot * gate_sigma).astype(BF16)
    gate_in_grad = (glu_cot * glu_value.astype(F32) * gate_sigma * (1.0 - gate_sigma)).astype(BF16)
    return (gate_grad[None], up_grad[None], down_grad[None], proj_grad, value_grad, gate_in_grad)


def solution(mesh):
    in_specs = (
        P("sp", None),
        P("sp", None),
        P("sp", None),
        P("sp", None),
        P("sp", None, "tp"),
        P("sp", None, "tp"),
        P("sp", "tp", None),
        P(None, "tp"),
        P("tp"),
        P(None, "tp"),
        P("tp", "sp"),
        P("tp", "sp"),
        P("tp", "sp"),
        P("sp"),
        P("sp"),
    )
    out_specs = (
        P("sp", None, "tp"),
        P("sp", None, "tp"),
        P("sp", "tp", None),
        P("sp", "tp"),
        P("tp", "sp"),
        P("tp", "sp"),
    )
    return jax.shard_map(
        on_device, mesh=mesh, in_specs=in_specs, out_specs=out_specs, check_vma=False
    )
```

time: 377 us -> 145 us (0.38)
  the two profiles are of different devices: /device:TPU:24 before, /device:TPU:1 now
where the time goes in v2:
time: 145 us
  Pallas kernels  109 us (75%)
  waiting for transfers between devices  12.9 us (9%)
  starting transfers between devices  9.58 us (7%)
  local copies, waits for them, and re-layouts  8.51 us (6%)
  matrix products  3.2 us (2%)
    pallas_call x1, Pallas kernels, experts(): pl.pallas_call(experts_kernel, out_shape=(jax.ShapeDtypeStruct((D, HIDDEN...  109 us
    unnamed x30, local copies, waits for them, and re-layouts  7.86 us
    all_to_all x1, waiting for transfers between devices, of_everyone(): lax.all_to_all(copies, axis, split_axis=0, concat_axis=0, tiled=True)  5.99 us
    ppermute x1, waiting for transfers between devices, from_behind(): return lax.ppermute(value, axis, pairs)  5.89 us
    all_to_all x1, starting transfers between devices, of_everyone(): lax.all_to_all(copies, axis, split_axis=0, concat_axis=0, tiled=True)  4.57 us
    all_to_all x1, starting transfers between devices, sent_and_summed(): lax.all_to_all(cut_along(value, dim, devices), axis, 0, 0, tiled=True)  3.72 us
    dot_general x2, matrix products, contract(): lax.dot_general(left, right, (((left_dim,), (right_dim,)), ((), ())), pre...  3.2 us
  transfers between devices with their start and end apart: 3, of which 3 were waited for; matrix products, arithmetic and copies ran while one was open for 3% of the time, Pallas kernels for 0%

profile of v2, /device:TPU:1, one launch (start us, length us, event | category | flops | bytes accessed | tf_op | source)
XLA Modules:
  0.0 145.0 jit_solution(5529392728463251987)
XLA Ops:
  0.6 0.0 copy-start
  0.6 1.0 copy.31
  1.7 0.0 copy-start.7
  1.7 0.0 copy-start.8
  1.7 0.0 copy-start.10
  1.7 108.6 %experts.1 = (bf16[2048,384]{1,0:T(8,128)(2,1)}, bf16[2048,384]{1,0:T(8,128)(2,1)}, bf16[384,2048]{1,0:T(8,128)(2,1)}, bf16[256,2048]{1,0:T(8,128)(2,1)}) custom-call(s32[2,256]{1,0:T(2,128)} %bitcast.94, f32[2,256]{1,0:T(2,128)} %bitcast.95, bf16[256,2048]{1,0:T(8,128)(2,1)} %in_ref.1, bf16[256,2048]{1,0:T(8,128)(2,1)} %cot_ref.1, ...), custom_call_target="tpu_custom_call" | custom-call | tf_op jit(solution)/shard_map/experts/pallas_call | solution.py:457
  110.3 0.0 copy-start.9
  110.3 0.0 copy-done
  110.3 0.0 copy-done.7
  110.3 0.0 copy-done.8
  110.3 0.0 copy-done.10
  110.3 1.8 %fusion.98 = (f32[256]{0:T(256)S(1)}, f32[256]{0:T(256)S(1)}, f32[128,256]{0,1:T(8,128)S(1)}) fusion(f32[256]{0:T(256)S(1)} %copy-done.7, f32[256]{0:T(256)S(1)} %copy-done.8, bf16[128,256]{0,1:T(8,128)(2,1)S(1)} %copy.31, f32[128]{0:T(128)S(1)} %copy-done.10, bf16[256,2048]{1,0:T(8,128)(2,1)} %get-tuple-element.13, bf16[2048,128]{1,0:T(8,128)(2,1)S(1)} %copy-done), kind=kOutput, calls=%fused_computation.201 | convolution fusion | flops 134741504 | bytes 1774080 | tf_op jit(solution)/shard_map/dot_general | solution.py:38
  112.2 0.0 copy-start.6
  112.2 0.6 broadcast_in_dim.20
  112.8 4.6 %all-to-all-start.1 = ((f32[16,2,256]{2,1,0:T(2,128)}), f32[16,2,256]{2,1,0:T(2,128)S(1)}, u32[]{:S(2)}, u32[]{:S(2)}) async-start(f32[16,2,256]{2,1,0:T(2,128)} %broadcast_in_dim.20), calls=%async_computation.1 | async-start | bytes 65536 | tf_op jit(solution)/shard_map/all_to_all | solution.py:523
  117.4 0.0 copy-done.9
  117.4 0.0 copy-start.4
  117.4 0.0 copy-start.5
  117.4 1.4 convolution_convert_fusion
  118.8 0.0 copy-done.6
  118.8 6.0 %all-to-all-done.1 = f32[16,2,256]{2,1,0:T(2,128)S(1)} async-done(((f32[16,2,256]{2,1,0:T(2,128)}), f32[16,2,256]{2,1,0:T(2,128)S(1)}, u32[]{:S(2)}, u32[]{:S(2)}) %all-to-all-start.1) | async-done | bytes 32800 | tf_op jit(solution)/shard_map/all_to_all | solution.py:523
  124.8 0.0 copy-start.3
  124.8 3.7 %all-to-all-start = ((bf16[16,128,128]{2,1,0:T(8,128)(2,1)}), bf16[16,128,128]{2,1,0:T(8,128)(2,1)S(1)}, u32[]{:S(2)}, u32[]{:S(2)}) async-start(bf16[16,128,128]{2,1,0:T(8,128)(2,1)} %bitcast.8), calls=%async_computation | async-start | bytes 1048576 | tf_op jit(solution)/shard_map/all_to_all | solution.py:517
  128.6 0.2 subtract_multiply_fusion
  128.8 1.3 collective-permute-start
  130.1 0.0 copy-done.4
  130.1 0.1 copy.33
  130.2 0.0 copy-done.5
  130.2 0.1 copy.34
  130.4 5.9 %collective-permute-done = f32[128,30]{0,1:T(8,128)S(1)} collective-permute-done((f32[128,30]{0,1:T(8,128)S(1)}, f32[128,30]{0,1:T(8,128)S(1)}, u32[]{:S(2)}, u32[]{:S(2)}) %collective-permute-start) | collective-permute-done | bytes 15392 | tf_op jit(solution)/shard_map/ppermute | solution.py:530
  136.3 0.4 multiply_convert_fusion
  136.7 0.7 copy.35
  137.5 0.7 copy.36
  138.2 1.0 all-to-all-done
  139.2 0.7 convert_reduce_fusion
  139.9 0.0 copy-done.3
  139.9 0.0 copy-start.2
  139.9 1.1 copy.43
  141.1 0.8 copy-done.2
  141.9 0.0 copy-start.1
  141.9 1.1 copy.44
  143.1 0.8 copy-done.1
  143.9 1.1 copy.45
  (7 shorter events, 0.1 us)
Async XLA Ops:
  0.6 109.7 %copy-start = (bf16[2048,128]{1,0:T(8,128)(2,1)S(1)}, bf16[2048,128]{1,0:T(8,128)(2,1)}, u32[]{:S(2)}) copy-start(bf16[2048,128]{1,0:T(8,128)(2,1)} %param.22) | copy-start | bytes 1572868
  1.7 108.7 %copy-start.7 = (f32[256]{0:T(256)S(1)}, f32[256]{0:T(256)}, u32[]{:S(2)}) copy-start(f32[256]{0:T(256)} %param.29) | copy-start | bytes 3076
  1.7 108.7 %copy-start.8 = (f32[256]{0:T(256)S(1)}, f32[256]{0:T(256)}, u32[]{:S(2)}) copy-start(f32[256]{0:T(256)} %param.28) | copy-start | bytes 3076
  1.7 108.7 %copy-start.10 = (f32[128]{0:T(128)S(1)}, f32[128]{0:T(128)}, u32[]{:S(2)}) copy-start(f32[128]{0:T(128)} %param.23) | copy-start | bytes 1540
  110.3 7.1 %copy-start.9 = (bf16[256,2048]{1,0:T(8,128)(2,1)S(1)}, bf16[256,2048]{1,0:T(8,128)(2,1)}, u32[]{:S(2)}) copy-start(bf16[256,2048]{1,0:T(8,128)(2,1)} %get-tuple-element.13) | copy-start | bytes 3145732
  112.2 6.6 %copy-start.6 = (f32[31,128]{1,0:T(8,128)S(1)}, f32[31,128]{1,0:T(8,128)}, u32[]{:S(2)}) copy-start(f32[31,128]{1,0:T(8,128)} %param.24) | copy-start | bytes 47620
  112.8 12.0 %all-to-all-start.1 = ((f32[16,2,256]{2,1,0:T(2,128)}), f32[16,2,256]{2,1,0:T(2,128)S(1)}, u32[]{:S(2)}, u32[]{:S(2)}) async-start(f32[16,2,256]{2,1,0:T(2,128)} %broadcast_in_dim.20), calls=%async_computation.1 | async-start | bytes 65536 | tf_op jit(solution)/shard_map/all_to_all | solution.py:523
  117.4 12.7 %copy-start.4 = (bf16[128,256]{1,0:T(8,128)(2,1)S(1)}, bf16[128,256]{1,0:T(8,128)(2,1)}, u32[]{:S(2)}) copy-start(bf16[128,256]{1,0:T(8,128)(2,1)} %param.26) | copy-start | bytes 196612
  117.4 12.8 %copy-start.5 = (bf16[128,256]{1,0:T(8,128)(2,1)S(1)}, bf16[128,256]{1,0:T(8,128)(2,1)}, u32[]{:S(2)}) copy-start(bf16[128,256]{1,0:T(8,128)(2,1)} %param.25) | copy-start | bytes 196612
  124.8 15.1 %copy-start.3 = (bf16[2048,384]{1,0:T(8,128)(2,1)S(1)}, bf16[2048,384]{1,0:T(8,128)(2,1)}, u32[]{:S(2)}) copy-start(bf16[2048,384]{1,0:T(8,128)(2,1)} %get-tuple-element.10) | copy-start | bytes 4718596
  124.8 14.4 %all-to-all-start = ((bf16[16,128,128]{2,1,0:T(8,128)(2,1)}), bf16[16,128,128]{2,1,0:T(8,128)(2,1)S(1)}, u32[]{:S(2)}, u32[]{:S(2)}) async-start(bf16[16,128,128]{2,1,0:T(8,128)(2,1)} %bitcast.8), calls=%async_computation | async-start | bytes 1048576 | tf_op jit(solution)/shard_map/all_to_all | solution.py:517
  128.8 7.5 %collective-permute-start = (f32[128,30]{0,1:T(8,128)S(1)}, f32[128,30]{0,1:T(8,128)S(1)}, u32[]{:S(2)}, u32[]{:S(2)}) collective-permute-start(f32[128,30]{0,1:T(8,128)S(1)} %slice.258), channel_id=1, source_target_pairs={{16,0},{32,16},{48,32},{64,48},{80,64},{96,80},{112,96},{128,112},... | collective-permute-start | bytes 46088 | tf_op jit(solution)/shard_map/ppermute | solution.py:530
  139.9 2.0 %copy-start.2 = (bf16[2048,384]{1,0:T(8,128)(2,1)S(1)}, bf16[2048,384]{1,0:T(8,128)(2,1)}, u32[]{:S(2)}) copy-start(bf16[2048,384]{1,0:T(8,128)(2,1)} %get-tuple-element.11) | copy-start | bytes 4718596
  141.9 2.0 %copy-start.1 = (bf16[384,2048]{1,0:T(8,128)(2,1)S(1)}, bf16[384,2048]{1,0:T(8,128)(2,1)}, u32[]{:S(2)}) copy-start(bf16[384,2048]{1,0:T(8,128)(2,1)} %get-tuple-element.12) | copy-start | bytes 4718596

commit v3 on v2

--- a/solution.py
+++ b/solution.py
@@ -26,6 +26,8 @@
 FAR_AT = N_OFF - len(FAR)
 HALVES = ((0, 3), (3, 2))
 ROWS = N_OFF * CAP
+EARLY = LOCAL + 1
+SPANS = ((0, EARLY * CAP), (EARLY * CAP, ROWS - EARLY * CAP))
 
 
 def sp_at(dy, dx):
@@ -117,6 +119,16 @@
     wg_ref,
     wu_ref,
     wd_ref,
+    wo_ref,
+    gain_ref,
+    conv_ref,
+    mean_ref,
+    rstd_ref,
+    gg_out,
+    ug_out,
+    dg_out,
+    cc_ref,
+    proj_ref,
     gg_ref,
     ug_ref,
     dg_ref,
@@ -141,14 +153,23 @@
     slots,
     chosen,
     mixed,
+    act,
+    factor,
+    centered,
+    total_out,
+    total_in,
+    proj_out,
+    proj_in,
+    rim,
     *sems,
 ):
-    (load_sem, *pairs) = sems
+    (load_sem, grad_sem, *pairs) = sems
+    grads = []
     (far_s, near_s, nshare_s, up_s, down_s, share_s, pair_s) = [
         (pairs[2 * i], pairs[2 * i + 1]) for i in range(7)
     ]
-    (rup_s, rdown_s, back_s, gup_s, gdown_s, gshare_s) = [
-        (pairs[2 * i], pairs[2 * i + 1]) for i in range(7, 13)
+    (rup_s, rdown_s, back_s, gup_s, gdown_s, gshare_s, total_s, proj_s, rim_s) = [
+        (pairs[2 * i], pairs[2 * i + 1]) for i in range(7, 16)
     ]
     sp, tp = lax.axis_index("sp"), lax.axis_index("tp")
     y, x = sp // SIDE, sp % SIDE
@@ -156,7 +177,8 @@
     partner = (sp, z * 2 + 1 - core)
     up = (sp, ((z + 1) % RING) * 2 + core)
     down = (sp, ((z + RING - 1) % RING) * 2 + core)
-    others = [partner, up, down]
+    n_tp = 2 * RING
+    others = [(sp, (tp + d) % n_tp) for d in range(1, n_tp)]
     others += [(sp_at(dy, dx), tp) for dy, dx in OFFSETS if (dy, dx) != (0, 0)]
     barrier = pltpu.get_barrier_semaphore()
     for device in others:
@@ -233,6 +255,20 @@
     send_near(8, 3)
     r[core, LOCAL] = x_near[LOCAL]
 
+    def prepare():
+        gain = gain_ref[...]
+        rstd = column(rstd_ref[...])
+        cent = (jnp.transpose(conv_ref[...].astype(F32)) - column(mean_ref[...])) * rstd
+        normed = cent * gain
+        sigma = jax.nn.sigmoid(normed)
+        centered[...] = cent
+        factor[...] = sigma * (1.0 + normed * (1.0 - sigma)) * gain
+        act[...] = jnp.transpose(normed * sigma).astype(BF16)
+        where = [column(value).astype(jnp.int32) for value in row_f]
+        for j in range(ROWS // 128):
+            at = lax.broadcasted_iota(jnp.int32, (tokens, 128), 1) + j * 128
+            chosen[:, pl.ds(j * 128, 128)] = ((where[0] == at) | (where[1] == at)).astype(BF16)
+
     def far(g, c, half):
         start, size = HALVES[half]
         return r.at[c, pl.ds(FAR_AT + start, size), g]
@@ -261,20 +297,101 @@
         ).astype(BF16)
         gu[span, pl.ds(HIDDEN, HIDDEN)] = (hidden_cot * gate_pre * sigma).astype(BF16)
 
+    def at_z(d):
+        return (z + RING + d) % RING
+
+    def span(half):
+        return pl.ds(*SPANS[half])
+
+    def chunk(d, half):
+        g = at_z(d)
+        total = contract(
+            gu[span(half), :], wgu[pl.ds(pl.multiple_of(g * 256, 256), 256), :], 1, 1
+        ).astype(BF16)
+        p[0, g, span(half), :] = total[:, :128]
+        p[1, g, span(half), :] = total[:, 128:]
+        copies.send(
+            p.at[1 - core, g, span(half)],
+            pair_buf.at[g, span(half)],
+            pair_s,
+            (d % RING, half),
+            partner,
+        )
+
+    def own(d, half):
+        g = at_z(d)
+        copies.arrived(pair_buf.at[g, span(half)], pair_s, (d % RING, half), partner)
+        return p[core, g, span(half), :].astype(F32) + pair_buf[g, span(half), :].astype(F32)
+
+    def came(buf, sem, hop, half):
+        copies.arrived(buf.at[hop, span(half)], sem, (hop, half), partner)
+        return buf[hop, span(half), :].astype(F32)
+
+    def step_up(hop, half):
+        total = own(4 - hop, half)
+        if hop > half:
+            total = total + came(in_up, rup_s, hop - 1, half)
+        out_up[hop, span(half), :] = total.astype(BF16)
+
+    def step_down(hop, half):
+        total = own(hop - 4, half)
+        if hop > 1 - half:
+            total = total + came(in_down, rdown_s, hop - 1, half)
+        out_down[hop, span(half), :] = total.astype(BF16)
+
+    def go_up(hop, half):
+        here = (hop, span(half))
+        copies.send(out_up.at[here], in_up.at[here], rup_s, (hop, half), up)
+
+    def go_down(hop, half):
+        here = (hop, span(half))
+        copies.send(out_down.at[here], in_down.at[here], rdown_s, (hop, half), down)
+
+    def weight_grads(i):
+        part = pl.ds(i * 256, 256)
+        rows_in = r[0, :, :, :, part].reshape(ROWS, 256)
+        rows_cot = r[1, :, :, :, part].reshape(ROWS, 256)
+        both = contract(rows_in, gu[...], 0, 0).astype(BF16)
+        gg_ref[part, :] = both[:, :HIDDEN]
+        ug_ref[part, :] = both[:, HIDDEN:]
+        dg_ref[:, part] = jnp.dot(hid_t[...], rows_cot, preferred_element_type=F32).astype(BF16)
+        for j, (buf, out, at) in enumerate(
+            ((gg_ref, gg_out, part), (ug_ref, ug_out, part), (dg_ref, dg_out, (slice(None), part)))
+        ):
+            grads.append(pltpu.make_async_copy(buf.at[at], out.at[at], grad_sem.at[i, j]))
+            grads[-1].start()
+
     def between(k):
         if k == 0:
-            forward(0, 4)
+            prepare()
             for load in loads:
                 load.wait()
+        if k == 1:
+            forward(0, 4)
+        if k == 2:
             shared(0, 4)
             forward_group(0, 4)
-        if k == 2:
+        if k == 3:
             forward(4, 5)
-        if k == 3:
             shared(4, 5)
             forward_group(4, 5)
+            chunk(4, 0)
+            chunk(-3, 0)
+            step_up(0, 0)
+            go_up(0, 0)
+            step_down(1, 0)
+            go_down(1, 0)
         if k == 4:
             forward(9, 2)
+            chunk(3, 0)
+            chunk(-2, 0)
+            step_up(1, 0)
+            go_up(1, 0)
+            step_down(2, 0)
+            go_down(2, 0)
+            chunk(2, 0)
+            chunk(-1, 0)
+            chunk(1, 0)
             shared(9, 2)
             forward_group(9, 2)
 
@@ -295,95 +412,39 @@
         between,
     )
     forward_group(FAR_AT, len(FAR))
-
-    half_rows = ROWS // 2
-
-    def at_z(d):
-        return (z + RING + d) % RING
-
-    def chunk(d):
-        g = at_z(d)
-        total = contract(
-            gu[...], wgu[pl.ds(pl.multiple_of(g * 256, 256), 256), :], 1, 1
-        ).astype(BF16)
-        p[0, g] = total[:, :128]
-        p[1, g] = total[:, 128:]
-        copies.send(p.at[1 - core, g], pair_buf.at[g], pair_s, d % RING, partner)
-
-    def paired(d):
-        copies.arrived(pair_buf.at[at_z(d)], pair_s, d % RING, partner)
-
-    def span(half):
-        return pl.ds(half * half_rows, half_rows)
-
-    def own(d, half):
-        g = at_z(d)
-        return p[core, g, span(half), :].astype(F32) + pair_buf[g, span(half), :].astype(F32)
-
-    def go(hop, half_up, half_down):
-        copies.send(
-            out_up.at[hop, span(half_up)], in_up.at[hop, span(half_up)], rup_s, (hop, half_up), up
-        )
-        copies.send(
-            out_down.at[hop, span(half_down)],
-            in_down.at[hop, span(half_down)],
-            rdown_s,
-            (hop, half_down),
-            down,
-        )
-
-    def came(buf, sem, hop, half):
-        copies.arrived(buf.at[hop, span(half)], sem, (hop, half), partner)
-        return buf[hop, span(half), :].astype(F32)
-
-    def weight_grads(i):
-        part = pl.ds(i * 256, 256)
-        rows_in = r[0, :, :, :, part].reshape(ROWS, 256)
-        rows_cot = r[1, :, :, :, part].reshape(ROWS, 256)
-        both = contract(rows_in, gu[...], 0, 0).astype(BF16)
-        gg_ref[part, :] = both[:, :HIDDEN]
-        ug_ref[part, :] = both[:, HIDDEN:]
-        dg_ref[:, part] = jnp.dot(hid_t[...], rows_cot, preferred_element_type=F32).astype(BF16)
-
-    chunk(4)
-    chunk(3)
-    paired(4)
-    out_up[0, span(0), :] = own(4, 0).astype(BF16)
-    out_down[0, span(1), :] = own(-4, 1).astype(BF16)
-    go(0, 0, 1)
-    chunk(-3)
-    paired(3)
-    paired(-3)
-    out_up[1, span(1), :] = own(3, 1).astype(BF16)
-    out_down[1, span(0), :] = own(-3, 0).astype(BF16)
-    go(1, 1, 0)
-    chunk(2)
-    chunk(-2)
-    for hop in range(1, 4):
-        d = 4 - hop
-        if hop > 1:
-            paired(d)
-            paired(-d)
-        out_up[hop, span(0), :] = (came(in_up, rup_s, hop - 1, 0) + own(d, 0)).astype(BF16)
-        out_down[hop, span(1), :] = (came(in_down, rdown_s, hop - 1, 1) + own(-d, 1)).astype(BF16)
-        go(hop, 0, 1)
-        if hop == 1:
-            chunk(1)
-            chunk(-1)
-        if hop > 1:
-            out_up[hop, span(1), :] = (came(in_up, rup_s, hop - 1, 1) + own(d, 1)).astype(BF16)
-            out_down[hop, span(0), :] = (came(in_down, rdown_s, hop - 1, 0) + own(-d, 0)).astype(
-                BF16
-            )
-            go(hop, 1, 0)
-        if hop == 2:
-            chunk(0)
-            hid_t[...] = jnp.transpose(hid[...])
-            weight_grads(0)
-        if hop == 3:
-            weight_grads(1)
-            weight_grads(2)
-    paired(0)
+    chunk(4, 1)
+    chunk(3, 1)
+    step_up(1, 1)
+    step_down(0, 1)
+    go_up(1, 1)
+    go_down(0, 1)
+    step_up(2, 0)
+    go_up(2, 0)
+    step_down(3, 0)
+    go_down(3, 0)
+    chunk(-3, 1)
+    chunk(2, 1)
+    step_down(1, 1)
+    go_down(1, 1)
+    step_up(2, 1)
+    go_up(2, 1)
+    step_up(3, 0)
+    go_up(3, 0)
+    chunk(-2, 1)
+    chunk(1, 1)
+    chunk(0, 0)
+    chunk(-1, 1)
+    chunk(0, 1)
+    hid_t[...] = jnp.transpose(hid[...])
+    step_down(2, 1)
+    go_down(2, 1)
+    step_up(3, 1)
+    go_up(3, 1)
+    weight_grads(0)
+    weight_grads(1)
+    step_down(3, 1)
+    go_down(3, 1)
+    weight_grads(2)
     for half in range(2):
         sums[span(half), :] = (
             own(0, half) + came(in_up, rup_s, 3, half) + came(in_down, rdown_s, 3, half)
@@ -395,10 +456,6 @@
             copies.send(sums.at[part], slots.at[part], back_s, o, (sp_at(-dy, -dx), tp))
     here = pl.ds(LOCAL * CAP, CAP)
     slots[here, :] = sums[here, :]
-    where = [column(value).astype(jnp.int32) for value in row_f]
-    for j in range(ROWS // 128):
-        at = lax.broadcasted_iota(jnp.int32, (tokens, 128), 1) + j * 128
-        chosen[:, pl.ds(j * 128, 128)] = ((where[0] == at) | (where[1] == at)).astype(BF16)
     weight_grads(3)
     weight_grads(4)
     for o in range(N_OFF):
@@ -439,10 +496,118 @@
         gshare_s,
         between_gather,
     )
+
+    act_cot = jnp.dot(m_ref[...], wo_ref[...], preferred_element_type=F32)
+    norm_cot = act_cot * factor[...]
+    for i, value in enumerate((norm_cot, norm_cot * centered[...])):
+        whole = jnp.broadcast_to(jnp.sum(value, axis=1, keepdims=True), (tokens, 128))
+        total_out[i : i + 1, :] = jnp.transpose(whole)[0:1, :]
+    total_in[tp] = total_out[...]
+    for d in range(1, n_tp):
+        copies.send(total_out, total_in.at[tp], total_s, d, (sp, (tp + d) % n_tp))
+    for s in range(N_OFF // 4):
+        part = jnp.dot(act[...], m_ref[:, pl.ds(s * 512, 512)], preferred_element_type=F32)
+        for i in range(4):
+            proj_out[4 * s + i] = part[:, i * 128 : i * 128 + 128].astype(BF16)
+    for o in range(N_OFF):
+        if o != LOCAL:
+            peer = sp_at(*OFFSETS[o])
+            copies.send(proj_out.at[peer], proj_in.at[o], proj_s, o, (peer, tp))
+    proj_in[LOCAL] = proj_out[sp]
+    for d in range(1, n_tp):
+        copies.arrived(total_in.at[(tp + n_tp - d) % n_tp], total_s, d, partner)
+    totals = jnp.sum(total_in[...], axis=0)
+    conv_cot = column(rstd_ref[...]) * (
+        norm_cot - column(totals[0:1, :]) / C - centered[...] * (column(totals[1:2, :]) / C)
+    )
+    cc_ref[pl.ds(0, tokens), :] = conv_cot
+    n_rim = rim.shape[1]
+    rim[0] = conv_cot[:n_rim, :]
+    copies.send(rim.at[0], rim.at[1], rim_s, 0, ((sp + N_OFF - 1) % N_OFF, tp))
+    for o in range(N_OFF):
+        if o != LOCAL:
+            copies.arrived(proj_in.at[o], proj_s, o, partner)
+    proj_ref[...] = jnp.sum(proj_in[...].astype(F32), axis=0)
+    copies.arrived(rim.at[1], rim_s, 0, partner)
+    cc_ref[pl.ds(tokens, n_rim), :] = jnp.where(sp == N_OFF - 1, 0.0, rim[1])
+    for grad in grads:
+        grad.wait()
     copies.finish()
 
 
-def experts(ids, weight, rows_in, cotangent, w_gate, w_up, w_down):
+def finish_kernel(
+    gg_ref,
+    ug_ref,
+    dg_ref,
+    cc_ref,
+    proj_ref,
+    taps_ref,
+    value_ref,
+    gate_ref,
+    gg_out,
+    ug_out,
+    dg_out,
+    proj_out,
+    value_out,
+    gate_out,
+    gg,
+    ug,
+    dg,
+    in_sem,
+    out_sem,
+):
+    takes, gives = [], []
+    for i, (src, buf, dst) in enumerate(
+        ((gg_ref, gg, gg_out), (ug_ref, ug, ug_out), (dg_ref, dg, dg_out))
+    ):
+        size = src.shape[0] // 2
+        for j in range(2):
+            part = pl.ds(j * size, size)
+            takes.append(pltpu.make_async_copy(src.at[part], buf.at[part], in_sem.at[i, j]))
+            gives.append(pltpu.make_async_copy(buf.at[part], dst.at[part], out_sem.at[i, j]))
+    for take in takes:
+        take.start()
+    tokens = value_ref.shape[1]
+    total = taps_ref[0:1, :] * cc_ref[pl.ds(0, tokens), :]
+    for lag in range(1, taps_ref.shape[0]):
+        total = total + taps_ref[lag : lag + 1, :] * cc_ref[pl.ds(lag, tokens), :]
+    for take, give in zip(takes, gives):
+        take.wait()
+        give.start()
+    glu_cot = jnp.transpose(total)
+    sigma = jax.nn.sigmoid(gate_ref[...].astype(F32))
+    value_out[...] = (glu_cot * sigma).astype(BF16)
+    gate_out[...] = (glu_cot * value_ref[...].astype(F32) * sigma * (1.0 - sigma)).astype(BF16)
+    proj_out[...] = jnp.transpose(proj_ref[...])
+    for give in gives:
+        give.wait()
+
+
+def finish(gg, ug, dg, cc, proj, taps, value, gate):
+    vmem = pl.BlockSpec(memory_space=pltpu.VMEM)
+    anywhere = pl.BlockSpec(memory_space=pl.ANY)
+
+    def like(a):
+        return jax.ShapeDtypeStruct(a.shape, a.dtype)
+
+    return pl.pallas_call(
+        finish_kernel,
+        out_shape=(like(gg), like(ug), like(dg), like(proj), like(value), like(value)),
+        in_specs=[anywhere] * 3 + [vmem] * 5,
+        out_specs=(anywhere,) * 3 + (vmem,) * 3,
+        scratch_shapes=[
+            *[pltpu.VMEM(a.shape, a.dtype) for a in (gg, ug, dg)],
+            pltpu.SemaphoreType.DMA((3, 2)),
+            pltpu.SemaphoreType.DMA((3, 2)),
+        ],
+        compiler_params=pltpu.CompilerParams(vmem_limit_bytes=60 << 20),
+        name="finish",
+    )(gg, ug, dg, cc, proj, taps, value, gate)
+
+
+def experts(
+    ids, weight, rows_in, cotangent, w_gate, w_up, w_down, w_out, gain, conv_out, mean, rstd, reach
+):
     dma = pltpu.SemaphoreType.DMA
     tokens = cotangent.shape[0]
     vmem = pl.BlockSpec(memory_space=pltpu.VMEM)
@@ -460,11 +625,16 @@
             jax.ShapeDtypeStruct((D, HIDDEN), BF16),
             jax.ShapeDtypeStruct((D, HIDDEN), BF16),
             jax.ShapeDtypeStruct((HIDDEN, D), BF16),
-            jax.ShapeDtypeStruct((tokens, D), BF16),
+            jax.ShapeDtypeStruct((tokens + reach, 128), F32),
+            jax.ShapeDtypeStruct((128, 128), F32),
         ),
-        in_specs=[vmem] * 4 + [anywhere] * 3,
-        out_specs=(vmem,) * 4,
+        in_specs=[vmem] * 4 + [anywhere] * 3 + [vmem] * 5,
+        out_specs=(anywhere,) * 3 + (vmem,) * 2,
         scratch_shapes=[
+            buf(D, HIDDEN),
+            buf(D, HIDDEN),
+            buf(HIDDEN, D),
+            buf(tokens, D),
             buf(tokens, D),
             buf(tokens, D),
             buf(len(FAR), 8, D),
@@ -485,49 +655,40 @@
             buf(ROWS, 128),
             buf(tokens, ROWS),
             buf(tokens, 128),
+            buf(128, tokens),
+            pltpu.VMEM((tokens, 128), F32),
+            pltpu.VMEM((tokens, 128), F32),
+            pltpu.VMEM((2, tokens), F32),
+            pltpu.VMEM((2 * RING, 2, tokens), F32),
+            buf(N_OFF, 128, 128),
+            buf(N_OFF, 128, 128),
+            pltpu.VMEM((2, reach, 128), F32),
             dma((3,)),
+            dma((RING, 3)),
             *both(len(FAR)),
             *both(FAR_AT),
             *both(FAR_AT),
             *both(4, 2),
             *both(4, 2),
             *both(RING, 2),
-            *both(RING),
+            *both(RING, 2),
             *both(4, 2),
             *both(4, 2),
             *both(N_OFF),
             *both(4, 2),
             *both(4, 2),
             *both(RING, 2),
+            *both(2 * RING),
+            *both(N_OFF),
+            *both(1),
         ],
         compiler_params=pltpu.CompilerParams(
             collective_id=0, has_side_effects=True, vmem_limit_bytes=60 << 20
         ),
         name="experts",
-    )(ids, weight, rows_in, cotangent, w_gate, w_up, w_down)
-
-
-def cut_along(value, dim, devices):
-    before, after = (value.shape[:dim], value.shape[dim + 1 :])
-    return jnp.moveaxis(value.reshape(*before, devices, -1, *after), dim, 0)
-
-
-def sent_and_summed(value, axis, dim):
-    devices = lax.axis_size(axis)
-    tiles = lax.all_to_all(cut_along(value, dim, devices), axis, 0, 0, tiled=True)
-    return jnp.sum(tiles.astype(F32), axis=0)
-
-
-def of_everyone(value, axis):
-    copies = jnp.broadcast_to(value, (lax.axis_size(axis), *value.shape))
-    everything = lax.all_to_all(copies, axis, split_axis=0, concat_axis=0, tiled=True)
-    return jnp.sum(everything, axis=0)
-
-
-def from_behind(value, axis, by):
-    devices = lax.axis_size(axis)
-    pairs = [(i, i + by) for i in range(devices) if 0 <= i + by < devices]
-    return lax.ppermute(value, axis, pairs)
+    )(
+        ids, weight, rows_in, cotangent, w_gate, w_up, w_down, w_out, gain, conv_out, mean, rstd
+    )
 
 
 def on_device(
@@ -547,35 +708,33 @@
     norm_mean,
     norm_rstd,
 ):
-    tokens_here = cotangent.shape[0]
-    gate_grad, up_grad, down_grad, mixed_cot = experts(
-        expert_ids.T, route_weight.T, saved_input, cotangent, w_gate[0], w_up[0], w_down[0]
-    )
-
-    centered = (conv_out.astype(F32) - norm_mean[None, :]) * norm_rstd[None, :]
-    normed = centered * channel_gain[:, None]
-    sigma = jax.nn.sigmoid(normed)
-    output_act = (normed * sigma).astype(BF16)
-    proj_grad = sent_and_summed(contract(mixed_cot, output_act, 0, 1).astype(BF16), "sp", 0)
-    act_cot = contract(w_out, mixed_cot, 0, 1)
-    norm_cot = act_cot * sigma * (1.0 + normed * (1.0 - sigma)) * channel_gain[:, None]
-    sums = of_everyone(
-        jnp.stack([jnp.sum(norm_cot, axis=0), jnp.sum(norm_cot * centered, axis=0)]), "tp"
-    )
-    first_sum, second_sum = sums[0], sums[1]
-    conv_cot = norm_rstd[None, :] * (
-        norm_cot - first_sum[None, :] / C - centered * second_sum[None, :] / C
-    )
-    reach = conv_taps.shape[0] - 1
-    rim = from_behind(conv_cot[:, :reach], "sp", -1)
-    padded = jnp.concatenate([conv_cot, rim], axis=1)
-    glu_cot = conv_taps[0][:, None] * padded[:, :tokens_here]
-    for lag in range(1, reach + 1):
-        glu_cot = glu_cot + conv_taps[lag][:, None] * padded[:, lag : lag + tokens_here]
-    gate_sigma = jax.nn.sigmoid(glu_gate.astype(F32))
-    value_grad = (glu_cot * gate_sigma).astype(BF16)
-    gate_in_grad = (glu_cot * glu_value.astype(F32) * gate_sigma * (1.0 - gate_sigma)).astype(BF16)
-    return (gate_grad[None], up_grad[None], down_grad[None], proj_grad, value_grad, gate_in_grad)
+    reach = 32
+    parts = experts(
+        expert_ids.T,
+        route_weight.T,
+        saved_input,
+        cotangent,
+        w_gate[0],
+        w_up[0],
+        w_down[0],
+        w_out,
+        channel_gain[None],
+        conv_out,
+        norm_mean[None],
+        norm_rstd[None],
+        reach,
+    )
+    gate_grad, up_grad, down_grad, proj_grad, value_grad, gate_in_grad = finish(
+        *parts, conv_taps, glu_value, glu_gate
+    )
+    return (
+        gate_grad[None],
+        up_grad[None],
+        down_grad[None],
+        proj_grad,
+        value_grad,
+        gate_in_grad,
+    )
 
 
 def solution(mesh):

time: 145 us -> 124 us (0.86)
  Pallas kernels: 109 us -> 123 us
  waiting for transfers between devices: 12.9 us -> 0 us
  starting transfers between devices: 9.58 us -> 0 us
  local copies, waits for them, and re-layouts: 8.51 us -> 0 us
  matrix products: 3.2 us -> 0 us
    pallas_call x1, Pallas kernels: 109 us -> 117 us  [experts(): pl.pallas_call(experts_kernel, out_shape=(jax.ShapeDtypeStruct((D, HIDDEN...]
    all_to_all x2 -> x0, starting transfers between devices: 8.29 us -> none  [the longest x1 4.57 us: of_everyone(): lax.all_to_all(copies, axis, split_axis=0, concat_axis=0, tiled=True)]
    unnamed x30 -> x0, local copies, waits for them, and re-layouts: 7.86 us -> none
    all_to_all x2 -> x0, waiting for transfers between devices: 7.02 us -> none  [the longest x1 5.99 us: of_everyone(): lax.all_to_all(copies, axis, split_axis=0, concat_axis=0, tiled=True)]
    ppermute x1 -> x0, waiting for transfers between devices: 5.89 us -> none  [from_behind(): return lax.ppermute(value, axis, pairs)]
    pallas_call x0 -> x1, Pallas kernels: none -> 5.63 us  [finish(): pl.pallas_call(finish_kernel, out_shape=(like(gg), like(ug), like(dg), li...]
    dot_general x2 -> x0, matrix products: 3.2 us -> none  [contract(): lax.dot_general(left, right, (((left_dim,), (right_dim,)), ((), ())), pre...]
  transfers between devices with their start and end apart: 3 -> 0, of which waited for: 3 -> 0; matrix products, arithmetic and copies ran while one was open for 3% -> 0% of each run, Pallas kernels for 0% -> 0%
where the time goes in v3:
time: 124 us
  Pallas kernels  123 us (99%)
    pallas_call x1, Pallas kernels, experts(): pl.pallas_call(experts_kernel, out_shape=(jax.ShapeDtypeStruct((D, HIDDEN...  117 us
    pallas_call x1, Pallas kernels, finish(): pl.pallas_call(finish_kernel, out_shape=(like(gg), like(ug), like(dg), li...  5.63 us

profile of v3, /device:TPU:1, one launch (start us, length us, event | category | flops | bytes accessed | tf_op | source)
XLA Modules:
  0.0 123.7 jit_solution(4844213392663012142)
XLA Ops:
  0.6 117.3 %experts.1 = (bf16[2048,384]{1,0:T(8,128)(2,1)}, bf16[2048,384]{1,0:T(8,128)(2,1)}, bf16[384,2048]{1,0:T(8,128)(2,1)}, f32[288,128]{1,0:T(8,128)}, f32[128,128]{1,0:T(8,128)}) custom-call(s32[2,256]{1,0:T(2,128)} %bitcast.14, f32[2,256]{1,0:T(2,128)} %bitcast.15, bf16[256,2048]{1,0:T(8,128)(2,1)} %in_ref.1, bf16[256,2048]{1,0:T(8,128)(2,1)} %cot_ref.1, ...), custom_call_target="tpu_custom_call" | custom-call | tf_op jit(solution)/shard_map/experts/pallas_call | solution.py:622
  118.0 5.6 %finish.1 = (bf16[2048,384]{1,0:T(8,128)(2,1)}, bf16[2048,384]{1,0:T(8,128)(2,1)}, bf16[384,2048]{1,0:T(8,128)(2,1)}, f32[128,128]{1,0:T(8,128)}, bf16[128,256]{1,0:T(8,128)(2,1)}, /*index=5*/bf16[128,256]{1,0:T(8,128)(2,1)}) custom-call(bf16[2048,384]{1,0:T(8,128)(2,1)} %get-tuple-element.17.gg_ref, bf16[2048,384]{1,0:T(8,128)(2,1)} %get-tuple-element.18.ug_ref, ...), custom_call_target="tpu_custom_call" | custom-call | tf_op jit(solution)/shard_map/finish/pallas_call | solution.py:593

commit v4 on v3

--- a/solution.py
+++ b/solution.py
@@ -20,14 +20,13 @@
 HERE = ((0, 0),)
 ACROSS = ((0, 2), (2, 0))
 FAR = ((1, 2), (3, 2), (2, 1), (2, 3), (2, 2))
-OFFSETS = NEXT + CORNER + HERE + ACROSS + FAR
+OFFSETS = NEXT + ACROSS + HERE + CORNER + FAR
 N_OFF = len(OFFSETS)
 LOCAL = OFFSETS.index((0, 0))
 FAR_AT = N_OFF - len(FAR)
 HALVES = ((0, 3), (3, 2))
 ROWS = N_OFF * CAP
-EARLY = LOCAL + 1
-SPANS = ((0, EARLY * CAP), (EARLY * CAP, ROWS - EARLY * CAP))
+SPANS = ((0, 7 * CAP), (7 * CAP, 4 * CAP), (11 * CAP, 5 * CAP))
 
 
 def sp_at(dy, dx):
@@ -112,23 +111,32 @@
 
 
 def experts_kernel(
+    ids_in,
+    weight_in,
+    rows_in_ref,
+    cot_in,
+    wg_ref,
+    wu_ref,
+    wd_ref,
+    wo_in,
+    gain_in,
+    conv_in,
+    mean_in,
+    rstd_in,
+    gg_out,
+    ug_out,
+    dg_out,
+    cc_ref,
+    proj_ref,
     ids_ref,
     weight_ref,
     in_ref,
     cot_ref,
-    wg_ref,
-    wu_ref,
-    wd_ref,
     wo_ref,
     gain_ref,
     conv_ref,
     mean_ref,
     rstd_ref,
-    gg_out,
-    ug_out,
-    dg_out,
-    cc_ref,
-    proj_ref,
     gg_ref,
     ug_ref,
     dg_ref,
@@ -161,9 +169,28 @@
     proj_out,
     proj_in,
     rim,
+    blocks,
     *sems,
 ):
     (load_sem, grad_sem, *pairs) = sems
+    firsts = [
+        pltpu.make_async_copy(src, dst, load_sem.at[3 + i])
+        for i, (src, dst) in enumerate(
+            (
+                (ids_in, ids_ref),
+                (weight_in, weight_ref),
+                (cot_in, cot_ref),
+                (rows_in_ref, in_ref),
+                (conv_in, conv_ref),
+                (mean_in, mean_ref),
+                (rstd_in, rstd_ref),
+                (gain_in, gain_ref),
+                (wo_in, wo_ref),
+            )
+        )
+    ]
+    for first in firsts:
+        first.start()
     grads = []
     (far_s, near_s, nshare_s, up_s, down_s, share_s, pair_s) = [
         (pairs[2 * i], pairs[2 * i + 1]) for i in range(7)
@@ -194,6 +221,8 @@
     for load in loads:
         load.start()
 
+    for first in firsts[:2]:
+        first.wait()
     n_experts = N_OFF
     expert = lax.broadcasted_iota(jnp.int32, (n_experts, tokens), 0)
     one = [(ids_ref[k : k + 1, :] == expert).astype(F32) for k in range(2)]
@@ -214,6 +243,8 @@
     def column(value):
         return jnp.transpose(jnp.broadcast_to(value, (128, tokens)))
 
+    for first in firsts[2:4]:
+        first.wait()
     for k, src in enumerate((src0, src1)):
         scale = column(weight_ref[k : k + 1, :])
         for j in range(D // 128):
@@ -248,14 +279,16 @@
         copies.send(
             x_far.at[i], r.at[core, FAR_AT + i, z], far_s, i, (sp_at(*offset), tp)
         )
-    fill(4, 4)
+    fill(4, 3)
     send_near(0, 4)
-    fill(8, 3)
-    send_near(4, 4)
-    send_near(8, 3)
+    fill(7, 4)
+    send_near(4, 3)
+    send_near(7, 4)
     r[core, LOCAL] = x_near[LOCAL]
 
     def prepare():
+        for first in firsts[4:]:
+            first.wait()
         gain = gain_ref[...]
         rstd = column(rstd_ref[...])
         cent = (jnp.transpose(conv_ref[...].astype(F32)) - column(mean_ref[...])) * rstd
@@ -329,13 +362,13 @@
 
     def step_up(hop, half):
         total = own(4 - hop, half)
-        if hop > half:
+        if hop > min(half, 1):
             total = total + came(in_up, rup_s, hop - 1, half)
         out_up[hop, span(half), :] = total.astype(BF16)
 
     def step_down(hop, half):
         total = own(hop - 4, half)
-        if hop > 1 - half:
+        if hop > 1 - min(half, 1):
             total = total + came(in_down, rdown_s, hop - 1, half)
         out_down[hop, span(half), :] = total.astype(BF16)
 
@@ -372,9 +405,9 @@
             shared(0, 4)
             forward_group(0, 4)
         if k == 3:
-            forward(4, 5)
-            shared(4, 5)
-            forward_group(4, 5)
+            forward(4, 3)
+            shared(4, 3)
+            forward_group(4, 3)
             chunk(4, 0)
             chunk(-3, 0)
             step_up(0, 0)
@@ -382,7 +415,6 @@
             step_down(1, 0)
             go_down(1, 0)
         if k == 4:
-            forward(9, 2)
             chunk(3, 0)
             chunk(-2, 0)
             step_up(1, 0)
@@ -392,8 +424,23 @@
             chunk(2, 0)
             chunk(-1, 0)
             chunk(1, 0)
-            shared(9, 2)
-            forward_group(9, 2)
+            forward(7, 4)
+            shared(7, 4)
+            forward_group(7, 4)
+            chunk(4, 1)
+            chunk(3, 1)
+            step_down(0, 1)
+            go_down(0, 1)
+            step_up(1, 1)
+            go_up(1, 1)
+
+    def hop_on(ups, downs):
+        for hop, half in ups:
+            step_up(hop, half)
+            go_up(hop, half)
+        for hop, half in downs:
+            step_down(hop, half)
+            go_down(hop, half)
 
     for i in range(len(FAR)):
         copies.arrived(r.at[core, FAR_AT + i, z], far_s, i, partner)
@@ -412,40 +459,34 @@
         between,
     )
     forward_group(FAR_AT, len(FAR))
-    chunk(4, 1)
-    chunk(3, 1)
-    step_up(1, 1)
-    step_down(0, 1)
-    go_up(1, 1)
-    go_down(0, 1)
-    step_up(2, 0)
-    go_up(2, 0)
-    step_down(3, 0)
-    go_down(3, 0)
+    chunk(4, 2)
+    chunk(3, 2)
+    hop_on(((1, 2),), ((0, 2),))
+    hop_on(((2, 0),), ((3, 0),))
     chunk(-3, 1)
     chunk(2, 1)
-    step_down(1, 1)
-    go_down(1, 1)
-    step_up(2, 1)
-    go_up(2, 1)
-    step_up(3, 0)
-    go_up(3, 0)
+    hop_on(((2, 1),), ((1, 1),))
+    chunk(-3, 2)
+    chunk(2, 2)
+    hop_on(((2, 2),), ((1, 2),))
+    hop_on(((3, 0),), ())
     chunk(-2, 1)
     chunk(1, 1)
-    chunk(0, 0)
+    hop_on(((3, 1),), ((2, 1),))
+    chunk(-2, 2)
+    chunk(1, 2)
+    hop_on(((3, 2),), ((2, 2),))
     chunk(-1, 1)
-    chunk(0, 1)
+    chunk(-1, 2)
     hid_t[...] = jnp.transpose(hid[...])
-    step_down(2, 1)
-    go_down(2, 1)
-    step_up(3, 1)
-    go_up(3, 1)
     weight_grads(0)
+    hop_on((), ((3, 1),))
+    hop_on((), ((3, 2),))
+    for half in range(3):
+        chunk(0, half)
     weight_grads(1)
-    step_down(3, 1)
-    go_down(3, 1)
     weight_grads(2)
-    for half in range(2):
+    for half in range(3):
         sums[span(half), :] = (
             own(0, half) + came(in_up, rup_s, 3, half) + came(in_down, rdown_s, 3, half)
         ).astype(BF16)
@@ -468,14 +509,11 @@
     half_tokens = tokens // 2
 
     def block(g, c, half):
-        return m_ref.at[
-            pl.ds(half * half_tokens, half_tokens),
-            pl.ds(pl.multiple_of((g * 2 + c) * 128, 128), 128),
-        ]
+        return blocks.at[g * 2 + c, pl.ds(half * half_tokens, half_tokens)]
 
     def between_gather(k):
         if k == 0:
-            m_ref[:, mine] = mixed[...]
+            blocks[tp] = mixed[...]
             weight_grads(5)
         if k == 1:
             weight_grads(6)
@@ -497,6 +535,8 @@
         between_gather,
     )
 
+    for j in range(n_tp):
+        m_ref[:, pl.ds(j * 128, 128)] = blocks[j]
     act_cot = jnp.dot(m_ref[...], wo_ref[...], preferred_element_type=F32)
     norm_cot = act_cot * factor[...]
     for i, value in enumerate((norm_cot, norm_cot * centered[...])):
@@ -628,9 +668,11 @@
             jax.ShapeDtypeStruct((tokens + reach, 128), F32),
             jax.ShapeDtypeStruct((128, 128), F32),
         ),
-        in_specs=[vmem] * 4 + [anywhere] * 3 + [vmem] * 5,
+        in_specs=[anywhere] * 12,
         out_specs=(anywhere,) * 3 + (vmem,) * 2,
         scratch_shapes=[
+            *[pltpu.VMEM(a.shape, a.dtype) for a in (ids, weight, rows_in, cotangent)],
+            *[pltpu.VMEM(a.shape, a.dtype) for a in (w_out, gain, conv_out, mean, rstd)],
             buf(D, HIDDEN),
             buf(D, HIDDEN),
             buf(HIDDEN, D),
@@ -663,7 +705,8 @@
             buf(N_OFF, 128, 128),
             buf(N_OFF, 128, 128),
             pltpu.VMEM((2, reach, 128), F32),
-            dma((3,)),
+            buf(2 * RING, tokens, 128),
+            dma((12,)),
             dma((RING, 3)),
             *both(len(FAR)),
             *both(FAR_AT),
@@ -671,9 +714,9 @@
             *both(4, 2),
             *both(4, 2),
             *both(RING, 2),
-            *both(RING, 2),
-            *both(4, 2),
-            *both(4, 2),
+            *both(RING, 3),
+            *both(4, 3),
+            *both(4, 3),
             *both(N_OFF),
             *both(4, 2),
             *both(4, 2),

time: 124 us -> 123 us (level)
  no operation moved by 1% of the time
where the time goes in v4:
time: 123 us
  Pallas kernels  122 us (99%)
    pallas_call x1, Pallas kernels, experts(): pl.pallas_call(experts_kernel, out_shape=(jax.ShapeDtypeStruct((D, HIDDEN...  116 us
    pallas_call x1, Pallas kernels, finish(): pl.pallas_call(finish_kernel, out_shape=(like(gg), like(ug), like(dg), li...  5.63 us

profile of v4, /device:TPU:1, one launch (start us, length us, event | category | flops | bytes accessed | tf_op | source)
XLA Modules:
  0.0 122.8 jit_solution(16318689072076871548)
XLA Ops:
  0.6 116.4 %experts.1 = (bf16[2048,384]{1,0:T(8,128)(2,1)}, bf16[2048,384]{1,0:T(8,128)(2,1)}, bf16[384,2048]{1,0:T(8,128)(2,1)}, f32[288,128]{1,0:T(8,128)}, f32[128,128]{1,0:T(8,128)}) custom-call(s32[2,256]{1,0:T(2,128)} %bitcast.14, f32[2,256]{1,0:T(2,128)} %bitcast.15, bf16[256,2048]{1,0:T(8,128)(2,1)} %rows_in_ref.1, bf16[256,2048]{1,0:T(8,128)(2,1)} %cot_in.1, ...), custom_call_target="tpu_custom_call" | custom-call | tf_op jit(solution)/shard_map/experts/pallas_call | solution.py:662
  117.0 5.6 %finish.1 = (bf16[2048,384]{1,0:T(8,128)(2,1)}, bf16[2048,384]{1,0:T(8,128)(2,1)}, bf16[384,2048]{1,0:T(8,128)(2,1)}, f32[128,128]{1,0:T(8,128)}, bf16[128,256]{1,0:T(8,128)(2,1)}, /*index=5*/bf16[128,256]{1,0:T(8,128)(2,1)}) custom-call(bf16[2048,384]{1,0:T(8,128)(2,1)} %get-tuple-element.17.gg_ref, bf16[2048,384]{1,0:T(8,128)(2,1)} %get-tuple-element.18.ug_ref, ...), custom_call_target="tpu_custom_call" | custom-call | tf_op jit(solution)/shard_map/finish/pallas_call | solution.py:633

commit v5 on v4

--- a/solution.py
+++ b/solution.py
@@ -515,10 +515,6 @@
         if k == 0:
             blocks[tp] = mixed[...]
             weight_grads(5)
-        if k == 1:
-            weight_grads(6)
-        if k == 2:
-            weight_grads(7)
 
     spread_ring(
         copies,
@@ -537,14 +533,6 @@
 
     for j in range(n_tp):
         m_ref[:, pl.ds(j * 128, 128)] = blocks[j]
-    act_cot = jnp.dot(m_ref[...], wo_ref[...], preferred_element_type=F32)
-    norm_cot = act_cot * factor[...]
-    for i, value in enumerate((norm_cot, norm_cot * centered[...])):
-        whole = jnp.broadcast_to(jnp.sum(value, axis=1, keepdims=True), (tokens, 128))
-        total_out[i : i + 1, :] = jnp.transpose(whole)[0:1, :]
-    total_in[tp] = total_out[...]
-    for d in range(1, n_tp):
-        copies.send(total_out, total_in.at[tp], total_s, d, (sp, (tp + d) % n_tp))
     for s in range(N_OFF // 4):
         part = jnp.dot(act[...], m_ref[:, pl.ds(s * 512, 512)], preferred_element_type=F32)
         for i in range(4):
@@ -554,6 +542,16 @@
             peer = sp_at(*OFFSETS[o])
             copies.send(proj_out.at[peer], proj_in.at[o], proj_s, o, (peer, tp))
     proj_in[LOCAL] = proj_out[sp]
+    act_cot = jnp.dot(m_ref[...], wo_ref[...], preferred_element_type=F32)
+    norm_cot = act_cot * factor[...]
+    for i, value in enumerate((norm_cot, norm_cot * centered[...])):
+        whole = jnp.broadcast_to(jnp.sum(value, axis=1, keepdims=True), (tokens, 128))
+        total_out[i : i + 1, :] = jnp.transpose(whole)[0:1, :]
+    total_in[tp] = total_out[...]
+    for d in range(1, n_tp):
+        copies.send(total_out, total_in.at[tp], total_s, d, (sp, (tp + d) % n_tp))
+    weight_grads(6)
+    weight_grads(7)
     for d in range(1, n_tp):
         copies.arrived(total_in.at[(tp + n_tp - d) % n_tp], total_s, d, partner)
     totals = jnp.sum(total_in[...], axis=0)

time: 123 us -> 122 us (level)
  no operation moved by 1% of the time
where the time goes in v5:
time: 122 us
  Pallas kernels  121 us (99%)
    pallas_call x1, Pallas kernels, experts(): pl.pallas_call(experts_kernel, out_shape=(jax.ShapeDtypeStruct((D, HIDDEN...  116 us
    pallas_call x1, Pallas kernels, finish(): pl.pallas_call(finish_kernel, out_shape=(like(gg), like(ug), like(dg), li...  5.63 us

profile of v5, /device:TPU:1, one launch (start us, length us, event | category | flops | bytes accessed | tf_op | source)
XLA Modules:
  0.0 122.2 jit_solution(17044024784142427938)
XLA Ops:
  0.6 115.7 %experts.1 = (bf16[2048,384]{1,0:T(8,128)(2,1)}, bf16[2048,384]{1,0:T(8,128)(2,1)}, bf16[384,2048]{1,0:T(8,128)(2,1)}, f32[288,128]{1,0:T(8,128)}, f32[128,128]{1,0:T(8,128)}) custom-call(s32[2,256]{1,0:T(2,128)} %bitcast.14, f32[2,256]{1,0:T(2,128)} %bitcast.15, bf16[256,2048]{1,0:T(8,128)(2,1)} %rows_in_ref.1, bf16[256,2048]{1,0:T(8,128)(2,1)} %cot_in.1, ...), custom_call_target="tpu_custom_call" | custom-call | tf_op jit(solution)/shard_map/experts/pallas_call | solution.py:660
  116.4 5.6 %finish.1 = (bf16[2048,384]{1,0:T(8,128)(2,1)}, bf16[2048,384]{1,0:T(8,128)(2,1)}, bf16[384,2048]{1,0:T(8,128)(2,1)}, f32[128,128]{1,0:T(8,128)}, bf16[128,256]{1,0:T(8,128)(2,1)}, /*index=5*/bf16[128,256]{1,0:T(8,128)(2,1)}) custom-call(bf16[2048,384]{1,0:T(8,128)(2,1)} %get-tuple-element.17.gg_ref, bf16[2048,384]{1,0:T(8,128)(2,1)} %get-tuple-element.18.ug_ref, ...), custom_call_target="tpu_custom_call" | custom-call | tf_op jit(solution)/shard_map/finish/pallas_call | solution.py:631
